TPU v7x, 32 devices: a whole 2x2x4 slice. The times are simulated.
32 devices in a mesh: grp: 2 (over y), sp: 4 (over z), tp: 4 (over x, core).
Axes of the slice: x: 2, y: 2, z: 4, core: 2. Of those that a mesh axis runs over, the one named last changes fastest.
Arguments:
- latent: bfloat16 [2048, 4096], P(('grp', 'sp')), parts along dimension 0, may hold values from -6 to 6
- context: bfloat16 [512, 4096], P(('grp', 'sp')), parts along dimension 0, may hold values from -6 to 6
- cond_latent: float32 [8192], P(('grp', 'sp')), parts along dimension 0, may hold values from -6 to 6
- cond_context: float32 [8192], P(('grp', 'sp')), parts along dimension 0, may hold values from -6 to 6
- mod_weight: bfloat16 [3, 4096, 4096], P(None, 'sp', 'tp'), may hold values from -0.09375 to 0.09375
- norm_gain: float32 [4096], replicated, may hold values from 0.1 to 1.9
- w_query: bfloat16 [4096, 1024], P('sp', 'tp'), may hold values from -0.09375 to 0.09375
- w_key: bfloat16 [4096, 1024], P('sp', 'tp'), may hold values from -0.09375 to 0.09375
- w_value: bfloat16 [4096, 2048], P('sp', 'tp'), may hold values from -0.09375 to 0.09375
- w_rank: bfloat16 [2, 4096, 64], P(None, 'sp'), may hold values from -0.09375 to 0.09375
- w_decay: bfloat16 [2, 64, 1024], P(None, None, 'tp'), may hold values from -0.75 to 0.75
- decay_bias: float32 [2, 1024], P(None, 'tp'), may hold values from -1 to 20
- decay_shift: float32 [2048, 16], P(('grp', 'sp'), 'tp'), parts along dimension 0, may hold values from -1 to 0
- out_gain: float32 [2048], P('tp'), may hold values from 0.1 to 1.9
- w_out: bfloat16 [2048, 4096], P('tp', 'sp'), may hold values from -0.125 to 0.125
Outputs:
- mixed: bfloat16 [2048, 4096], P(('grp', 'sp')), parts along dimension 0
There are 2 independent parts, one for each index of `grp`. A program takes and returns all parts, laid end to end along the dimension named above; an argument that names none is the same for every part. Nothing has to cross between parts.
All inputs are finite; a program needn't handle non-finite values.
Results may differ from a plain program's by a relative error of at most 0.0095.
Values may be sent and summed in bfloat16 or wider, within the bound.
A program may use at most 128 MiB of HBM per device.

v0:
```python
import jax
import jax.numpy as jnp
from jax import lax
from jax.sharding import PartitionSpec as P

DK = 64
DV = 128
BLOCK = 64


eps = 1e-06
normalizer = 16.0
precise = lax.Precision.HIGHEST


def carried_in(array, axis, join, neutral, backward):
    count = lax.axis_size(axis)
    place = lax.axis_index(axis)
    ahead = count - 1 - place if backward else place
    gathered = jax.tree.map(
        lambda a, kind: lax.all_gather(a.astype(kind), axis),
        array,
        jax.tree.map(lambda a: jnp.bfloat16 if a.dtype == jnp.float32 else a.dtype, array),
    )
    state = jax.tree.map(lambda a, e: jnp.zeros_like(a) + jnp.asarray(e, a.dtype), array, neutral)

    def one(turn, state):
        source = count - 1 - turn if backward else turn
        return join(
            state,
            jax.tree.map(
                lambda a, own: lax.dynamic_index_in_dim(a, source, 0, False).astype(own.dtype),
                gathered,
                array,
            ),
        )

    return lax.fori_loop(0, ahead, one, state)


def rounded(tensor):
    return lax.optimization_barrier(tensor.astype(jnp.bfloat16))


def modulated(tokens, norm_gain, shift_row, scale_row):
    widened = tokens.astype(jnp.float32)
    normalized = widened * lax.rsqrt(jnp.mean(widened * widened, axis=-1, keepdims=True) + eps)
    return (normalized * norm_gain * (1.0 + scale_row) + shift_row).astype(jnp.bfloat16)


def project(tokens, weight):
    return rounded(jnp.dot(tokens, weight, preferred_element_type=jnp.float32))


def log_decay(rank_rows, weight, bias):
    return (
        jax.nn.log_sigmoid(jnp.dot(rank_rows, weight, preferred_element_type=jnp.float32) + bias)
        / normalizer
    )


def by_heads(tensor, width):
    return tensor.astype(jnp.float32).reshape(tensor.shape[0], -1, width)


def context_state(key_rows, value_rows, decays, forward):
    running = jnp.cumsum(decays, axis=0)
    if forward:
        factor = jnp.exp(running[-1] - running)
    else:
        factor = jnp.exp(running - decays)
    return jnp.einsum("thd,the->hde", key_rows * factor, value_rows, precision=precise)


def chained(earlier, later):
    return (earlier[0] + later[0], jnp.exp(later[0])[:, :, None] * earlier[1] + later[1])


def segment_chain(queries, key_rows, value_rows, decays):
    length, head_count, width = queries.shape
    blocks = length // BLOCK
    lower_mask = jnp.tril(jnp.ones((BLOCK, BLOCK), dtype=bool))

    def in_blocks(tensor):
        return tensor.reshape(blocks, BLOCK, head_count, tensor.shape[-1])

    def advance(carry, inputs):
        carry_state, offset = carry
        query_block, key_block, value_block, decay_block = inputs
        running = jnp.cumsum(decay_block, axis=0)
        carried = jnp.einsum(
            "chd,hde->che", query_block * jnp.exp(running), carry_state, precision=precise
        )
        flat_running = running.reshape(BLOCK, head_count * width)
        relative = jnp.where(
            lower_mask[:, :, None], flat_running[:, None] - flat_running[None, :], -jnp.inf
        )
        products = (
            jnp.exp(relative) * query_block.reshape(BLOCK, 1, -1) * key_block.reshape(1, BLOCK, -1)
        )
        scores = products.reshape(BLOCK, BLOCK, head_count, width).sum(axis=-1)
        within = jnp.einsum("ijh,jhe->ihe", scores, value_block, precision=precise)
        block_total = running[-1]
        carry_state = jnp.exp(block_total)[:, :, None] * carry_state + jnp.einsum(
            "chd,che->hde",
            key_block * jnp.exp(block_total - running),
            value_block,
            precision=precise,
        )
        lifted = query_block * jnp.exp(offset + running)
        return ((carry_state, offset + block_total), (carried + within, lifted))

    initial = (
        jnp.zeros((head_count, width, value_rows.shape[-1]), jnp.float32),
        jnp.zeros((head_count, width), jnp.float32),
    )
    (final_state, totals), (outputs, lifted) = lax.scan(
        advance,
        initial,
        (in_blocks(queries), in_blocks(key_rows), in_blocks(value_rows), in_blocks(decays)),
    )
    return (
        outputs.reshape(length, head_count, -1),
        lifted.reshape(length, head_count, width),
        (totals, final_state),
    )


def local(
    latent,
    context,
    cond_latent,
    cond_context,
    mod_weight,
    norm_gain,
    w_query,
    w_key,
    w_value,
    w_rank,
    w_decay,
    decay_bias,
    decay_shift,
    out_gain,
    w_out,
):
    silu_latent = jax.nn.silu(cond_latent).astype(jnp.bfloat16)
    silu_context = jax.nn.silu(cond_context).astype(jnp.bfloat16)
    term_latent = jnp.einsum(
        "d,rdc->rc", silu_latent, mod_weight, preferred_element_type=jnp.float32
    )
    term_context = jnp.einsum(
        "d,rdc->rc", silu_context, mod_weight[:2], preferred_element_type=jnp.float32
    )
    terms = jnp.concatenate([term_latent, term_context], axis=0)
    summed_terms = lax.psum(terms, "sp")
    modulation = lax.all_gather(summed_terms, "tp", axis=1, tiled=True)
    query_all, key_all, value_all, rank_all, output_all, context_rows = (
        lax.all_gather(w_query, "sp", axis=0, tiled=True),
        lax.all_gather(w_key, "sp", axis=0, tiled=True),
        lax.all_gather(w_value, "sp", axis=0, tiled=True),
        lax.all_gather(w_rank, "sp", axis=1, tiled=True),
        lax.all_gather(w_out, "sp", axis=1, tiled=True),
        lax.all_gather(context, "sp", axis=0, tiled=True),
    )
    h_latent = modulated(latent, norm_gain, modulation[0], modulation[1])
    h_context = modulated(context_rows, norm_gain, modulation[3], modulation[4])
    queries = by_heads(project(h_latent, query_all), DK)
    key_rows = by_heads(project(h_latent, key_all), DK)
    value_rows = by_heads(project(h_latent, value_all), DV)
    shift_rows = decay_shift[:, :, None]
    log_fwd = (
        by_heads(log_decay(project(h_latent, rank_all[0]), w_decay[0], decay_bias[0]), DK)
        + shift_rows
    )
    log_bwd = (
        by_heads(log_decay(project(h_latent, rank_all[1]), w_decay[1], decay_bias[1]), DK)
        + shift_rows
    )
    context_keys = by_heads(project(h_context, key_all), DK)
    context_values = by_heads(project(h_context, value_all), DV)
    context_fwd = by_heads(
        log_decay(project(h_context, rank_all[0]), w_decay[0], decay_bias[0]), DK
    )
    context_bwd = by_heads(
        log_decay(project(h_context, rank_all[1]), w_decay[1], decay_bias[1]), DK
    )
    own_fwd = (
        jnp.sum(context_fwd, axis=0),
        context_state(context_keys, context_values, context_fwd, True),
    )
    own_bwd = (
        jnp.sum(context_bwd, axis=0),
        context_state(context_keys, context_values, context_bwd, False),
    )
    out_fwd, lift_fwd, pair_fwd = segment_chain(queries, key_rows, value_rows, log_fwd)
    flipped_out, flipped_lift, pair_bwd = segment_chain(
        jnp.flip(queries, 0), jnp.flip(key_rows, 0), jnp.flip(value_rows, 0), jnp.flip(log_bwd, 0)
    )
    out_bwd = jnp.flip(flipped_out, 0)
    lift_bwd = jnp.flip(flipped_lift, 0)
    zero_pair = (jnp.zeros_like(pair_fwd[0]), jnp.zeros_like(pair_fwd[1]))
    before = carried_in(pair_fwd, "sp", chained, zero_pair, False)
    after = carried_in(pair_bwd, "sp", chained, zero_pair, True)
    start_fwd = own_fwd[1]
    start_bwd = own_bwd[1]
    entry_forward = chained((zero_pair[0], start_fwd), before)[1]
    entry_bwd = chained((zero_pair[0], start_bwd), after)[1]
    combined = (
        out_fwd
        + out_bwd
        + jnp.einsum("thd,hde->the", lift_fwd, entry_forward, precision=precise)
        + jnp.einsum("thd,hde->the", lift_bwd, entry_bwd, precision=precise)
    )
    combined = combined * lax.rsqrt(jnp.mean(combined * combined, axis=-1, keepdims=True) + eps)
    normed = (combined.reshape(combined.shape[0], -1) * out_gain).astype(jnp.bfloat16)
    partial_out = jnp.dot(normed, output_all, preferred_element_type=jnp.float32)
    summed = lax.psum(partial_out.astype(jnp.bfloat16), "tp").astype(jnp.float32)
    return (latent.astype(jnp.float32) + modulation[2] * summed).astype(jnp.bfloat16)


def solution(mesh):
    return jax.shard_map(
        local,
        mesh=mesh,
        in_specs=(
            P(("grp", "sp"), None),
            P(("grp", "sp"), None),
            P(("grp", "sp")),
            P(("grp", "sp")),
            P(None, "sp", "tp"),
            P(),
            P("sp", "tp"),
            P("sp", "tp"),
            P("sp", "tp"),
            P(None, "sp", None),
            P(None, None, "tp"),
            P(None, "tp"),
            P(("grp", "sp"), "tp"),
            P("tp"),
            P("tp", "sp"),
        ),
        out_specs=P(("grp", "sp"), None),
        check_vma=False,
    )
```

profile of v0, /device:TPU:0, one launch (start us, length us, event | category | flops | bytes accessed | tf_op | source)
XLA Modules:
  0.0 493.2 jit_solution(15336666345237326209)
XLA Ops:
  11.5 4.1 fusion.104
  16.3 22.4 %psum.14 = f32[5,1024]{1,0:T(8,128)S(1)} all-reduce(f32[5,1024]{1,0:T(8,128)S(1)} %pad_maximum_fusion), channel_id=1, replica_groups=mesh['grp'=2,'sp'=4,'tp'=4] {'sp'}, use_global_device_ids=true, to_apply=%region_0.1 | all-reduce | flops 5120 | bytes 40960 | tf_op jit(solution)/shard_map/psum | solution.py:155
  38.7 5.4 %all_gather.45 = f32[5,4096]{1,0:T(8,128)S(1)} all-gather(f32[5,1024]{1,0:T(8,128)S(1)} %psum.14), channel_id=1, replica_groups=mesh['grp'=2,'sp'=4,'tp'=4] {'tp'}, dimensions={1}, use_global_device_ids=true | all-gather | bytes 102400 | tf_op jit(solution)/shard_map/all_gather | solution.py:156
  46.0 12.3 %all-gather.21.cloned.1.call-done = bf16[256,4096]{1,0:T(8,128)(2,1)} async-done(((bf16[64,4096]{1,0:T(8,128)(2,1)}), bf16[256,4096]{1,0:T(8,128)(2,1)}) %all-gather.21.cloned.1.call-update) | async-done | bytes 2097168 | tf_op jit(solution)/shard_map/all_gather | solution.py:163
  58.4 2.1 fusion.48
  60.5 5.6 %fusion.52 = (bf16[256,4096]{1,0:T(8,128)(2,1)}, bf16[256,4096]{1,0:T(8,128)(2,1)}) fusion(bf16[256,4096]{1,0:T(8,128)(2,1)} %all-gather.21.cloned.1.call-done, f32[4096]{0:T(1024)S(1)} %bitcast.327, f32[4096]{0:T(1024)S(1)} %bitcast.328, f32[256]{0:T(256)S(1)} %add_rsqrt_fusion.1, f32[4096]{0:T(1024)S(1)} %copy-done.11, f32[4096]{0:T(1024)S(1)} %bitcast.329, ...), kind=kLoop, calls=%fused_computation.88 | loop fusion | flops 12582912 | bytes 8472576 | tf_op jit(solution)/shard_map/convert_element_type | solution.py:48
  66.0 38.3 %all-gather.15.cloned.1.call-done = bf16[4096,256]{1,0:T(8,128)(2,1)} async-done(((bf16[1024,256]{1,0:T(8,128)(2,1)}), bf16[4096,256]{1,0:T(8,128)(2,1)}) %all-gather.15.cloned.1.call-update) | async-done | bytes 2097168 | tf_op jit(solution)/shard_map/all_gather | solution.py:159
  104.4 2.9 convolution_convert_fusion.5
  108.5 42.0 %all-gather.19.cloned.1.call-done = bf16[4096,256]{1,0:T(8,128)(2,1)} async-done(((bf16[1024,256]{1,0:T(8,128)(2,1)}), bf16[4096,256]{1,0:T(8,128)(2,1)}) %all-gather.19.cloned.1.call-update) | async-done | bytes 2097168 | tf_op jit(solution)/shard_map/all_gather | solution.py:158
  150.4 2.9 convolution_convert_fusion.4
  154.4 24.3 %all-gather.13.cloned.1.call-done = bf16[2,4096,64]{1,2,0:T(8,128)(2,1)} async-done(((bf16[2,1024,64]{1,2,0:T(8,128)(2,1)}), bf16[2,4096,64]{1,2,0:T(8,128)(2,1)}) %all-gather.13.cloned.1.call-update) | async-done | bytes 1048592 | tf_op jit(solution)/shard_map/all_gather | solution.py:161
  178.7 2.4 convolution_convert_fusion.8
  189.6 2.4 convolution_convert_fusion.6
  194.1 4.5 reduce-window.16
  198.9 3.6 convolution_convert_fusion.3
  202.5 1.7 copy.149
  204.2 2.5 convolution_convert_fusion.9
  208.9 2.4 convolution_convert_fusion.7
  212.6 2.4 reduce-window.14
  216.2 2.2 broadcast_add_fusion
  218.4 41.9 %all-gather.17.cloned.1.call-done = bf16[4096,512]{1,0:T(8,128)(2,1)} async-done(((bf16[1024,512]{1,0:T(8,128)(2,1)}), bf16[4096,512]{1,0:T(8,128)(2,1)}) %all-gather.17.cloned.1.call-update) | async-done | bytes 4194320 | tf_op jit(solution)/shard_map/all_gather | solution.py:160
  260.2 4.1 convolution_convert_fusion.2
  266.2 4.8 rev.22
  272.7 43.7 %while.63 = (s32[]{:T(128)}, f32[4,64,128]{2,1,0:T(8,128)S(1)}, f32[4,64]{1,0:T(4,128)S(1)}, f32[4,64,4,128]{3,1,0,2:T(8,128)}, f32[4,64,4,64]{3,2,1,0:T(4,128)}...) while((s32[]{:T(128)}, f32[4,64,128]{2,1,0:T(8,128)S(1)}, ...), condition=%wide.region_9.10_spmd.clone, body=%wide.region_6.9_spmd.clone.sunk | while | flops 82006528 | bytes 2839165 | solution.py:117
  274.8 3.7 multiply_reduce_fusion.6
  285.7 3.7 multiply_reduce_fusion.6
  296.6 3.7 multiply_reduce_fusion.6
  303.8 1.6 fusion.174
  307.6 3.7 multiply_reduce_fusion.6
  316.4 8.6 %all-gather.5 = bf16[4,4,64]{2,1,0:T(4,128)(2,1)S(1)} all-gather(bf16[1,4,64]{2,1,0:T(4,128)(2,1)S(1)} %convert_bitcast_fusion.1), channel_id=4, replica_groups=mesh['grp'=2,'sp'=4,'tp'=4] {'sp'}, dimensions={0}, use_global_device_ids=true | all-gather | bytes 2560 | tf_op jit(solution)/shard_map/all_gather | solution.py:21
  326.8 36.2 %while.62 = (s32[]{:T(128)}, f32[4,64,128]{2,1,0:T(8,128)S(1)}, f32[4,64]{1,0:T(4,128)S(1)}, f32[4,64,4,128]{3,1,0,2:T(8,128)}, f32[4,64,4,64]{3,2,1,0:T(4,128)}...) while((s32[]{:T(128)}, f32[4,64,128]{2,1,0:T(8,128)S(1)}, ...), condition=%wide.region_5.6_spmd.clone, body=%wide.region_2.5_spmd.clone.sunk | while | flops 82006528 | bytes 3034753 | solution.py:117
  328.8 3.7 multiply_reduce_fusion.5
  337.9 3.7 multiply_reduce_fusion.5
  346.9 3.7 multiply_reduce_fusion.5
  355.9 3.7 multiply_reduce_fusion.5
  362.9 14.2 %all-gather.3 = bf16[16,64,128]{2,1,0:T(8,128)(2,1)S(1)} all-gather(bf16[4,64,128]{2,1,0:T(8,128)(2,1)S(1)} %convert_element_type.142), channel_id=5, replica_groups=mesh['grp'=2,'sp'=4,'tp'=4] {'sp'}, dimensions={0}, use_global_device_ids=true | all-gather | bytes 327680 | tf_op jit(solution)/shard_map/all_gather | solution.py:21
  377.7 4.8 convolution_convert_fusion.1
  382.6 8.3 %all-gather.4 = bf16[4,4,64]{2,1,0:T(4,128)(2,1)S(1)} all-gather(bf16[1,4,64]{2,1,0:T(4,128)(2,1)S(1)} %convert_bitcast_fusion.2), channel_id=2, replica_groups=mesh['grp'=2,'sp'=4,'tp'=4] {'sp'}, dimensions={0}, use_global_device_ids=true | all-gather | bytes 2560 | tf_op jit(solution)/shard_map/all_gather | solution.py:21
  390.8 14.5 %all-gather.1 = bf16[16,64,128]{2,1,0:T(8,128)(2,1)} all-gather(bf16[4,64,128]{2,1,0:T(8,128)(2,1)S(1)} %convert_element_type.135), channel_id=3, replica_groups=mesh['grp'=2,'sp'=4,'tp'=4] {'sp'}, dimensions={0}, use_global_device_ids=true | all-gather | bytes 327680 | tf_op jit(solution)/shard_map/all_gather | solution.py:21
  405.4 2.0 copy.147
  407.4 5.0 %rev.24 = f32[256,4,128]{0,2,1:T(8,128)} reverse(f32[256,4,128]{0,2,1:T(8,128)} %copy.147), dimensions={0} | reverse | bytes 1048576 | tf_op jit(solution)/shard_map/jit(_flip)/rev | solution.py:199
  412.5 2.0 copy.148
  414.5 2.0 copy.161
  416.5 1.8 rev.25
  421.0 2.0 fusion.62
  423.9 4.8 convolution_convert_fusion
  428.8 53.9 %all-reduce.2.cloned.1.call-done = bf16[256,4096]{1,0:T(8,128)(2,1)} async-done(((bf16[256,4096]{1,0:T(8,128)(2,1)}), bf16[256,4096]{1,0:T(8,128)(2,1)}) %all-reduce.2.cloned.1.call-update) | async-done | bytes 2097168 | tf_op jit(solution)/shard_map/psum | solution.py:217
  482.7 3.7 fusion.58
  (221 shorter events, 82.8 us)
Async XLA Ops:
  6.5 51.8 %all-gather.21.cloned.1.call-start = ((), (), s32[]{:S(2)}) async-start(), calls=%async_computation.4 | async-start | bytes 2621440 | tf_op jit(solution)/shard_map/all_gather | solution.py:163
  7.3 97.1 %all-gather.15.cloned.1.call-start = ((), (), s32[]{:S(2)}) async-start(), calls=%async_computation.1 | async-start | bytes 2621440 | tf_op jit(solution)/shard_map/all_gather | solution.py:159
  8.0 142.4 %all-gather.19.cloned.1.call-start = ((), (), s32[]{:S(2)}) async-start(), calls=%async_computation.3 | async-start | bytes 2621440 | tf_op jit(solution)/shard_map/all_gather | solution.py:158
  8.7 169.9 %all-gather.13.cloned.1.call-start = ((), (), s32[]{:S(2)}) async-start(), calls=%async_computation | async-start | bytes 1310720 | tf_op jit(solution)/shard_map/all_gather | solution.py:161
  9.3 6.3 %copy-start.14 = (f32[1024]{0:T(1024)S(1)}, f32[1024]{0:T(1024)}, u32[]{:S(2)}) copy-start(f32[1024]{0:T(1024)} %param.26) | copy-start | bytes 12292
  9.3 250.9 %all-gather.17.cloned.1.call-start = ((), (), s32[]{:S(2)}) async-start(), calls=%async_computation.2 | async-start | bytes 5242880 | tf_op jit(solution)/shard_map/all_gather | solution.py:160
  9.9 414.0 %all-gather.23.cloned.1.call-start = ((), (), s32[]{:S(2)}) async-start(), calls=%async_computation.5 | async-start | bytes 5242880 | tf_op jit(solution)/shard_map/all_gather | solution.py:162
  10.5 472.2 %all-reduce.2.cloned.1.call-start = ((), (), s32[]{:S(2)}) async-start(), calls=%async_computation.6 | async-start | bytes 4194304 | tf_op jit(solution)/shard_map/psum | solution.py:217
  10.6 5.0 %copy-start.1 = (bf16[3,1024,1024]{2,1,0:T(8,128)(2,1)S(1)}, bf16[3,1024,1024]{2,1,0:T(8,128)(2,1)}, u32[]{:S(2)}) copy-start(bf16[3,1024,1024]{2,1,0:T(8,128)(2,1)} %param.27) | copy-start | bytes 18874372
  11.4 33.3 %copy-start = (bf16[256,4096]{1,0:T(8,128)(2,1)S(1)}, bf16[256,4096]{1,0:T(8,128)(2,1)}, u32[]{:S(2)}) copy-start(bf16[256,4096]{1,0:T(8,128)(2,1)} %param.23) | copy-start | bytes 6291460
  15.6 29.7 %copy-start.16 = (f32[2,256]{1,0:T(2,128)S(1)}, f32[2,256]{1,0:T(2,128)}, u32[]{:S(2)}) copy-start(f32[2,256]{1,0:T(2,128)} %param.34) | copy-start | bytes 6148
  15.6 30.3 %copy-start.12 = (f32[256,4]{0,1:T(4,128)S(1)}, f32[256,4]{0,1:T(4,128)}, u32[]{:S(2)}) copy-start(f32[256,4]{0,1:T(4,128)} %param.35) | copy-start | bytes 12292
  15.6 44.8 %copy-start.11 = (f32[4096]{0:T(1024)S(1)}, f32[4096]{0:T(1024)}, u32[]{:S(2)}) copy-start(f32[4096]{0:T(1024)} %param.28) | copy-start | bytes 49156
  108.5 72.7 %copy-start.18 = (bf16[2,64,256]{2,1,0:T(8,128)(2,1)S(1)}, bf16[2,64,256]{2,1,0:T(8,128)(2,1)}, u32[]{:S(2)}) copy-start(bf16[2,64,256]{2,1,0:T(8,128)(2,1)} %param.33) | copy-start | bytes 196612
  193.3 13.4 %copy-start.4 = (f32[256,256]{0,1:T(8,128)}, f32[256,256]{0,1:T(8,128)S(1)}, u32[]{:S(2)}) copy-start(f32[256,256]{0,1:T(8,128)S(1)} %copy.157) | copy-start | bytes 786436
  194.1 12.6 %copy-start.17 = (f32[1,256]{1,0:T(1,128)S(1)}, f32[1,256]{1,0:T(1,128)}, u32[]{:S(2)}) copy-start(f32[1,256]{1,0:T(1,128)} %get-tuple-element.477) | copy-start | bytes 3076
  198.6 9.2 %copy-start.6 = (f32[64,4,2,128]{3,0,1,2:T(8,128)}, f32[64,4,2,128]{3,0,1,2:T(8,128)S(1)}, u32[]{:S(2)}) copy-start(f32[64,4,2,128]{3,0,1,2:T(8,128)S(1)} %reduce-window.16) | copy-start | bytes 786436
  215.0 49.3 %copy-start.2 = (f32[64,4,2,128]{3,0,1,2:T(8,128)}, f32[64,4,2,128]{3,0,1,2:T(8,128)S(1)}, u32[]{:S(2)}) copy-start(f32[64,4,2,128]{3,0,1,2:T(8,128)S(1)} %reduce-window.14) | copy-start | bytes 786436
  382.5 35.8 %copy-start.3 = (f32[64,4,2,128]{3,0,1,2:T(8,128)S(1)}, f32[64,4,2,128]{3,0,1,2:T(8,128)}, u32[]{:S(2)}) copy-start(f32[64,4,2,128]{3,0,1,2:T(8,128)} %copy-done.2) | copy-start | bytes 786436
  382.5 35.8 %copy-start.8 = (f32[256,256]{0,1:T(8,128)S(1)}, f32[256,256]{0,1:T(8,128)}, u32[]{:S(2)}) copy-start(f32[256,256]{0,1:T(8,128)} %copy.149) | copy-start | bytes 786436
  382.5 35.8 %copy-start.13 = (f32[4,64]{1,0:T(4,128)S(1)}, f32[4,64]{1,0:T(4,128)}, u32[]{:S(2)}) copy-start(f32[4,64]{1,0:T(4,128)} %slice_reduce_fusion.2) | copy-start | bytes 3076
  382.5 37.1 %copy-start.5 = (f32[256,256]{0,1:T(8,128)S(1)}, f32[256,256]{0,1:T(8,128)}, u32[]{:S(2)}) copy-start(f32[256,256]{0,1:T(8,128)} %copy-done.4) | copy-start | bytes 786436
  382.5 37.1 %copy-start.7 = (f32[64,4,2,128]{3,0,1,2:T(8,128)S(1)}, f32[64,4,2,128]{3,0,1,2:T(8,128)}, u32[]{:S(2)}) copy-start(f32[64,4,2,128]{3,0,1,2:T(8,128)} %copy-done.6) | copy-start | bytes 786436
  414.5 9.2 %copy-start.15 = (f32[512]{0:T(512)S(1)}, f32[512]{0:T(512)}, u32[]{:S(2)}) copy-start(f32[512]{0:T(512)} %param.36) | copy-start | bytes 6148
  418.2 4.8 copy-start.9
  423.9 58.7 %copy-start.10 = (f32[1,4096]{1,0:T(1,128)S(1)}, f32[1,4096]{1,0:T(1,128)}, u32[]{:S(2)}) copy-start(f32[1,4096]{1,0:T(1,128)} %get-tuple-element.469) | copy-start | bytes 49156
Sparse Core Ops, SparseCore 0:
  8.9 49.4 all-gather.20
  59.9 44.3 all-gather.14
  105.9 44.4 all-gather.18
  151.9 26.7 all-gather.12
  180.1 80.1 all-gather.16
  261.7 79.2 all-gather.22
  428.9 53.7 all-reduce.1
where the time goes:
time: 496 us; the launch traced here: 493 us
  waiting for transfers between devices  216 us (44%)
  other arithmetic  80.4 us (16%)
  blocking collectives  73.4 us (15%)
  matrix products  67.4 us (14%)
  local copies, waits for them, and re-layouts  40.8 us (8%)
  between operations  14 us (3%)
    psum x1, waiting for transfers between devices, local(): lax.psum(partial_out.astype(jnp.bfloat16), 'tp').astype(jnp.float32)  53.9 us
    all_gather x4, blocking collectives, carried_in(): lax.all_gather(a.astype(kind), axis)  45.6 us
    all_gather x1, waiting for transfers between devices, local(): lax.all_gather(w_query, 'sp', axis=0, tiled=True)  42 us
    all_gather x1, waiting for transfers between devices, local(): lax.all_gather(w_value, 'sp', axis=0, tiled=True)  41.9 us
    all_gather x1, waiting for transfers between devices, local(): lax.all_gather(w_key, 'sp', axis=0, tiled=True)  38.3 us
    reduce_sum x8, other arithmetic, advance(): scores = products.reshape(BLOCK, BLOCK, head_count, width).sum(axis=-1)  29.9 us
    dot_general x9, matrix products, project(): return rounded(jnp.dot(tokens, weight, preferred_element_type=jnp.float32))  28.1 us
    all_gather x1, waiting for transfers between devices, local(): lax.all_gather(w_rank, 'sp', axis=1, tiled=True)  24.3 us
  transfers between devices with their start and end apart: 7, of which 6 were waited for; matrix products, arithmetic and copies ran while one was open for 37% of the time, Pallas kernels for 0%

commit v1 on v0

--- a/solution.py
+++ b/solution.py
@@ -1,6 +1,10 @@
+import functools
+
 import jax
 import jax.numpy as jnp
 from jax import lax
+from jax.experimental import pallas as pl
+from jax.experimental.pallas import tpu as pltpu
 from jax.sharding import PartitionSpec as P
 
 DK = 64
@@ -218,9 +222,343 @@
     return (latent.astype(jnp.float32) + modulation[2] * summed).astype(jnp.bfloat16)
 
 
+MESH = pl.DeviceIdType.MESH
+SUB = 16
+
+
+def exchange_kernel(axis, count, sends, *refs):
+    total = len(sends)
+    sources, targets = refs[:total], refs[total : 2 * total]
+    send_sem, recv_sem, own_sem = refs[2 * total :]
+    me = lax.axis_index(axis)
+    barrier = pltpu.get_barrier_semaphore()
+    for step in range(1, count):
+        pl.semaphore_signal(
+            barrier, inc=1, device_id={axis: lax.rem(me + step, count)}, device_id_type=MESH
+        )
+    pl.semaphore_wait(barrier, count - 1)
+    copies = []
+    for item in range(total):
+        for step in range(1, count):
+            peer = lax.rem(me + step, count)
+            copy = pltpu.make_async_remote_copy(
+                src_ref=sources[item].at[peer] if sends[item] else sources[item],
+                dst_ref=targets[item].at[me],
+                send_sem=send_sem.at[item, step - 1],
+                recv_sem=recv_sem.at[item, step - 1],
+                device_id={axis: peer},
+                device_id_type=MESH,
+            )
+            copy.start()
+            copies.append(copy)
+    for item in range(total):
+        copy = pltpu.make_async_copy(
+            sources[item].at[me] if sends[item] else sources[item],
+            targets[item].at[me],
+            own_sem.at[item],
+        )
+        copy.start()
+        copies.append(copy)
+    for copy in copies:
+        copy.wait()
+
+
+def exchange(axis, collective, *items):
+    count = lax.axis_size(axis)
+    sends = tuple(scatter for _, scatter in items)
+    arrays = [array for array, _ in items]
+    shapes = [
+        jax.ShapeDtypeStruct(a.shape if s else (count,) + a.shape, a.dtype) for a, s in items
+    ]
+    return pl.pallas_call(
+        functools.partial(exchange_kernel, axis, count, sends),
+        out_shape=shapes,
+        in_specs=[pl.BlockSpec(memory_space=pltpu.VMEM)] * len(items),
+        out_specs=[pl.BlockSpec(memory_space=pltpu.VMEM)] * len(items),
+        scratch_shapes=[
+            pltpu.SemaphoreType.DMA((len(items), count - 1)),
+            pltpu.SemaphoreType.DMA((len(items), count - 1)),
+            pltpu.SemaphoreType.DMA((len(items),)),
+        ],
+        compiler_params=pltpu.CompilerParams(collective_id=collective, has_side_effects=True),
+        name=f"exchange_{collective}",
+    )(*arrays)
+
+
+def narrow_dot(left, right, dims):
+    return lax.dot_general(
+        left.astype(jnp.bfloat16),
+        right.astype(jnp.bfloat16),
+        (dims, ((), ())),
+        preferred_element_type=jnp.float32,
+    )
+
+
+def mix_kernel(q_ref, k_ref, v_ref, f_ref, b_ref, ck_ref, cv_ref, cf_ref, cb_ref, gain_ref, o_ref, later_ref):
+    length, width = q_ref.shape
+    depth = v_ref.shape[1]
+    row = lax.broadcasted_iota(jnp.int32, (BLOCK, BLOCK), 0)
+    column = lax.broadcasted_iota(jnp.int32, (BLOCK, BLOCK), 1)
+    lower = jnp.where(row >= column, 1.0, 0.0).astype(jnp.float32)
+    upper = jnp.where(row <= column, 1.0, 0.0).astype(jnp.float32)
+    key_row = lax.broadcasted_iota(jnp.int32, (BLOCK, width), 0)
+
+    def sums(ones, decays):
+        return jnp.dot(ones, decays, precision=precise, preferred_element_type=jnp.float32)
+
+    def step(state, keys, values, running, block_total):
+        return state * jnp.exp(block_total) + narrow_dot(
+            values, keys * jnp.exp(block_total - running), ((0,), (0,))
+        )
+
+    def at(ref, index):
+        return ref[pl.ds(pl.multiple_of(index * BLOCK, BLOCK), BLOCK), :].astype(jnp.float32)
+
+    zero = jnp.zeros((depth, width), jnp.float32)
+    context_blocks = ck_ref.shape[0] // BLOCK
+    blocks = length // BLOCK
+
+    def context_forward(index, state):
+        running = sums(lower, at(cf_ref, index))
+        return step(state, at(ck_ref, index), at(cv_ref, index), running, running[BLOCK - 1 :])
+
+    def context_backward(turn, state):
+        index = context_blocks - 1 - turn
+        running = sums(upper, at(cb_ref, index))
+        return step(state, at(ck_ref, index), at(cv_ref, index), running, running[:1])
+
+    start_fwd = lax.fori_loop(0, context_blocks, context_forward, zero)
+    start_bwd = lax.fori_loop(0, context_blocks, context_backward, zero)
+
+    def backward(turn, state):
+        index = blocks - 1 - turn
+        later_ref[index] = state
+        running = sums(upper, at(b_ref, index))
+        return step(state, at(k_ref, index), at(v_ref, index), running, running[:1])
+
+    lax.fori_loop(0, blocks, backward, start_bwd)
+
+    def forward(index, state):
+        queries, keys, values = at(q_ref, index), at(k_ref, index), at(v_ref, index)
+        ahead = sums(lower, at(f_ref, index))
+        behind = sums(upper, at(b_ref, index))
+        pieces = []
+        for sub in range(BLOCK // SUB):
+            low, high = sub * SUB, (sub + 1) * SUB
+            own = slice(low, high)
+            left, right = [], []
+            if low:
+                edge = ahead[low - 1 : low]
+                left.append(queries[own] * jnp.exp(ahead[own] - edge))
+                right.append(
+                    jnp.where(key_row < low, keys * jnp.exp(jnp.minimum(edge - ahead, 0.0)), 0.0)
+                )
+            if high < BLOCK:
+                edge = behind[high : high + 1]
+                left.append(queries[own] * jnp.exp(behind[own] - edge))
+                right.append(
+                    jnp.where(key_row >= high, keys * jnp.exp(jnp.minimum(edge - behind, 0.0)), 0.0)
+                )
+            piece = narrow_dot(left[0], right[0], ((1,), (1,)))
+            for one, other in zip(left[1:], right[1:]):
+                piece = piece + narrow_dot(one, other, ((1,), (1,)))
+            pieces.append(piece)
+        scores = jnp.concatenate(pieces, axis=0)
+
+        def cut(tensor):
+            return tensor.reshape(BLOCK // SUB, SUB, width)
+
+        q3, k3, a3, b3 = cut(queries), cut(keys), cut(ahead), cut(behind)
+        inner = lax.broadcasted_iota(jnp.int32, q3.shape, 1)
+        for other in range(SUB):
+            one = slice(other, other + 1)
+            relative = jnp.where(inner >= other, a3 - a3[:, one], b3 - b3[:, one])
+            product = jnp.exp(relative) * q3 * k3[:, one]
+            product = jnp.where(inner == other, 2.0 * product, product)
+            near = jnp.sum(product.reshape(BLOCK, width), axis=-1, keepdims=True)
+            scores = scores + jnp.where(column == (row // SUB) * SUB + other, near, 0.0)
+        output = (
+            narrow_dot(scores, values, ((1,), (0,)))
+            + narrow_dot(queries * jnp.exp(ahead), state, ((1,), (1,)))
+            + narrow_dot(queries * jnp.exp(behind), later_ref[index], ((1,), (1,)))
+        )
+        output = output * lax.rsqrt(jnp.mean(output * output, axis=-1, keepdims=True) + eps)
+        o_ref[pl.ds(pl.multiple_of(index * BLOCK, BLOCK), BLOCK), :] = (
+            output * gain_ref[...]
+        ).astype(o_ref.dtype)
+        return step(state, keys, values, ahead, ahead[BLOCK - 1 :])
+
+    lax.fori_loop(0, blocks, forward, start_fwd)
+
+
+def mix(queries, key_rows, value_rows, log_fwd, log_bwd, keys, values, fwd, bwd, gain):
+    length, width = queries.shape
+    depth = value_rows.shape[1]
+    return pl.pallas_call(
+        mix_kernel,
+        out_shape=jax.ShapeDtypeStruct((length, depth), jnp.bfloat16),
+        in_specs=[pl.BlockSpec(memory_space=pltpu.VMEM)] * 10,
+        out_specs=pl.BlockSpec(memory_space=pltpu.VMEM),
+        scratch_shapes=[pltpu.VMEM((length // BLOCK, depth, width), jnp.float32)],
+        name="mix",
+    )(queries, key_rows, value_rows, log_fwd, log_bwd, keys, values, fwd, bwd, gain)
+
+
+def local_heads(
+    latent,
+    context,
+    cond_latent,
+    cond_context,
+    mod_weight,
+    norm_gain,
+    w_query,
+    w_key,
+    w_value,
+    w_rank,
+    w_decay,
+    decay_bias,
+    decay_shift,
+    out_gain,
+    w_out,
+):
+    sp, tp = lax.axis_size("sp"), lax.axis_size("tp")
+    at_sp, at_tp = lax.axis_index("sp"), lax.axis_index("tp")
+    rows, model = latent.shape
+    context_rows = context.shape[0]
+    inner = model // sp
+    heads = w_query.shape[1] // DK
+    silu_latent = jax.nn.silu(cond_latent).astype(jnp.bfloat16)
+    silu_context = jax.nn.silu(cond_context).astype(jnp.bfloat16)
+    term_latent = jnp.einsum(
+        "d,rdc->rc", silu_latent, mod_weight, preferred_element_type=jnp.float32
+    )
+    term_context = jnp.einsum(
+        "d,rdc->rc", silu_context, mod_weight[:2], preferred_element_type=jnp.float32
+    )
+    terms = jnp.concatenate([term_latent, term_context], axis=0)
+
+    def inverse(tokens):
+        widened = tokens.astype(jnp.float32)
+        return lax.rsqrt(jnp.mean(widened * widened, axis=-1) + eps)
+
+    scales = jnp.concatenate([inverse(latent), inverse(context)])[None]
+
+    def share(tokens):
+        quarter = tokens.shape[0] // tp
+        own = lax.dynamic_slice_in_dim(tokens, at_tp * quarter, quarter, 0)
+        return own.reshape(quarter, sp, inner).transpose(1, 0, 2)
+
+    latent_share, context_share, terms_all, scales_all, shift_all = exchange(
+        "sp",
+        1,
+        (share(latent), True),
+        (share(context), True),
+        (terms, False),
+        (scales, False),
+        (decay_shift.T[:, None, :], True),
+    )
+    latent_all, context_all, modulation = exchange(
+        "tp",
+        2,
+        (latent_share, False),
+        (context_share, False),
+        (jnp.sum(terms_all, axis=0), False),
+    )
+    modulation = modulation.transpose(1, 0, 2).reshape(terms.shape[0], model)
+    own_mod = lax.dynamic_slice_in_dim(modulation, at_sp * inner, inner, 1)
+    own_gain = lax.dynamic_slice_in_dim(norm_gain, at_sp * inner, inner, 0)
+    raw_latent = latent_all.transpose(1, 0, 2, 3).reshape(sp * rows, inner)
+    raw_context = context_all.transpose(1, 0, 2, 3).reshape(sp * context_rows, inner)
+
+    def tokens_of(raw, inverses, shift_row, scale_row):
+        normalized = raw.astype(jnp.float32) * inverses.reshape(-1, 1)
+        return (normalized * own_gain * (1.0 + scale_row) + shift_row).astype(jnp.bfloat16)
+
+    h_latent = tokens_of(raw_latent, scales_all[:, 0, :rows], own_mod[0], own_mod[1])
+    h_context = tokens_of(raw_context, scales_all[:, 0, rows:], own_mod[3], own_mod[4])
+    h_all = jnp.concatenate([h_latent, h_context], axis=0)
+    weights = jnp.concatenate(
+        [
+            w_query.reshape(inner, heads, DK),
+            w_key.reshape(inner, heads, DK),
+            w_value.reshape(inner, heads, DV),
+        ],
+        axis=2,
+    ).transpose(1, 0, 2)
+    partial = jnp.einsum(
+        "tk,hkc->htc", h_all, weights, preferred_element_type=jnp.float32
+    ).astype(jnp.bfloat16)
+
+    def my_rows(tokens):
+        cut = tokens.reshape(sp, tp, -1, inner)
+        return lax.dynamic_index_in_dim(cut, at_tp, 1, False).reshape(-1, inner)
+
+    rank_rows = jnp.concatenate([my_rows(h_latent), my_rows(h_context)], axis=0)
+    rank_partial = jnp.dot(
+        rank_rows,
+        jnp.concatenate([w_rank[0], w_rank[1]], axis=1),
+        preferred_element_type=jnp.float32,
+    ).astype(jnp.bfloat16)
+    partial_all, rank_all = exchange("sp", 3, (partial, True), (rank_partial, False))
+    rank_own = jnp.sum(rank_all.astype(jnp.float32), axis=0).astype(jnp.bfloat16)
+    (rank_full,) = exchange("tp", 4, (rank_own, False))
+    width = rank_full.shape[-1]
+    cut = rank_rows.shape[0] - sp * context_rows // tp
+
+    def in_order(tensor):
+        return tensor.reshape(tp, sp, -1, width).transpose(1, 0, 2, 3).reshape(-1, width)
+
+    ranks = jnp.concatenate([in_order(rank_full[:, :cut]), in_order(rank_full[:, cut:])], axis=0)
+    joined = jnp.sum(partial_all.astype(jnp.float32), axis=0).astype(jnp.bfloat16)
+    own_decay = lax.dynamic_slice_in_dim(w_decay, at_sp * DK, DK, 2)
+    own_bias = lax.dynamic_slice_in_dim(decay_bias, at_sp * DK, DK, 1)
+    half = width // 2
+    fwd = log_decay(ranks[:, :half], own_decay[0], own_bias[0])
+    bwd = log_decay(ranks[:, half:], own_decay[1], own_bias[1])
+    span = sp * rows
+    shift_rows = shift_all.reshape(span, 1)
+    normed = mix(
+        joined[:span, :DK],
+        joined[:span, DK : 2 * DK],
+        joined[:span, 2 * DK :],
+        fwd[:span] + shift_rows,
+        bwd[:span] + shift_rows,
+        joined[span:, DK : 2 * DK],
+        joined[span:, 2 * DK :],
+        fwd[span:],
+        bwd[span:],
+        lax.dynamic_slice_in_dim(out_gain, at_sp * DV, DV, 0)[None],
+    )
+    (normed_all,) = exchange("sp", 5, (normed, False))
+    part = jnp.einsum(
+        "htc,hcd->td",
+        normed_all,
+        w_out.reshape(heads, DV, -1),
+        preferred_element_type=jnp.float32,
+    ).astype(jnp.bfloat16)
+    columns = part.shape[1] // tp
+    (part_all,) = exchange(
+        "tp", 6, (part.reshape(span, tp, columns).transpose(1, 0, 2), True)
+    )
+    summed = jnp.sum(part_all.astype(jnp.float32), axis=0)
+    gate = lax.dynamic_slice_in_dim(own_mod[2], at_tp * columns, columns, 0)
+    residual = lax.dynamic_slice_in_dim(raw_latent, at_tp * columns, columns, 1)
+    slab = (residual.astype(jnp.float32) + gate * summed).astype(jnp.bfloat16)
+    (slab_rows,) = exchange("sp", 7, (slab.reshape(sp, rows, columns), True))
+    (slab_all,) = exchange("tp", 8, (slab_rows, False))
+    return slab_all.transpose(2, 1, 0, 3).reshape(rows, model)
+
+
+def chosen(mesh, *arrays):
+    sizes = dict(mesh.shape)
+    heads = arrays[6].shape[1]
+    one_head_each = heads == DK * sizes["sp"] * sizes["tp"]
+    return local_heads if one_head_each else local
+
+
 def solution(mesh):
-    return jax.shard_map(
-        local,
+    return lambda *arrays: jax.shard_map(
+        chosen(mesh, *arrays),
         mesh=mesh,
         in_specs=(
             P(("grp", "sp"), None),
@@ -241,4 +579,4 @@
         ),
         out_specs=P(("grp", "sp"), None),
         check_vma=False,
-    )
+    )(*arrays)

time: 496 us -> 328 us (0.66)
  Pallas kernels: 0 us -> 256 us
  waiting for transfers between devices: 216 us -> 0 us
  blocking collectives: 73.4 us -> 0 us
  other arithmetic: 80.4 us -> 17.3 us
  matrix products: 67.4 us -> 14.3 us
  between operations: 14 us -> 0.35 us
    pallas_call x0 -> x9, Pallas kernels: none -> 256 us  [the longest x8 235 us: exchange(): pl.pallas_call(functools.partial(exchange_kernel, axis, count, sends), ou...]
    all_gather x6 -> x0, waiting for transfers between devices: 159 us -> none  [the longest x1 42 us: local(): lax.all_gather(w_query, 'sp', axis=0, tiled=True)]
    psum x1 -> x0, waiting for transfers between devices: 53.9 us -> none  [local(): lax.psum(partial_out.astype(jnp.bfloat16), 'tp').astype(jnp.float32)]
    all_gather x5 -> x0, blocking collectives: 51 us -> none  [the longest x4 45.6 us: carried_in(): lax.all_gather(a.astype(kind), axis)]
    dot_general x40 -> x5, matrix products: 63 us -> 13 us  [the longest x1 4.45 us: local_heads(): jnp.einsum('tk,hkc->htc', h_all, weights, preferred_element_type=jnp.floa...]
    psum x1 -> x0, blocking collectives: 22.4 us -> none  [local(): summed_terms = lax.psum(terms, 'sp')]
    reduce_sum x10 -> x6, other arithmetic: 32.5 us -> 10.9 us  [the longest x2 3.48 us: inverse(): return lax.rsqrt(jnp.mean(widened * widened, axis=-1) + eps)]
    another operation x13 -> x0, other arithmetic: 14.8 us -> none  [the longest x8 7.77 us: advance(): running = jnp.cumsum(decay_block, axis=0)]
  transfers between devices with their start and end apart: 7 -> 0, of which waited for: 6 -> 0; matrix products, arithmetic and copies ran while one was open for 37% -> 0% of each run, Pallas kernels for 0% -> 0%
where the time goes in v1:
time: 328 us; the launch traced here: 324 us
  Pallas kernels  256 us (78%)
  local copies, waits for them, and re-layouts  35.9 us (11%)
  other arithmetic  17.3 us (5%)
  matrix products  14.3 us (4%)
    pallas_call x8, Pallas kernels, exchange(): pl.pallas_call(functools.partial(exchange_kernel, axis, count, sends), ou...  235 us
    pallas_call x1, Pallas kernels, mix(): pl.pallas_call(mix_kernel, out_shape=jax.ShapeDtypeStruct((length, depth)...  21.6 us

profile of v1, /device:TPU:0, one launch (start us, length us, event | category | flops | bytes accessed | tf_op | source)
XLA Modules:
  0.0 324.4 jit_solution(3422839063455088133)
XLA Ops:
  0.0 1.2 copy-done
  1.2 1.3 dynamic-slice_bitcast_fusion.4.gain_ref
  2.6 1.2 multiply_reduce_fusion.1
  3.8 0.8 constant_dynamic-slice_fusion.1
  4.6 2.2 multiply_reduce_fusion
  7.5 0.7 dynamic_slice.40
  8.2 2.8 fusion
  11.7 0.9 fusion.43
  13.2 0.9 constant_dynamic-slice_fusion.4
  14.9 1.2 constant_dynamic-slice_fusion.5
  16.0 0.8 copy.55
  16.9 25.4 %exchange_1.1 = (bf16[4,64,1024]{2,1,0:T(8,128)(2,1)}, bf16[4,16,1024]{2,1,0:T(8,128)(2,1)}, f32[4,5,1024]{2,1,0:T(8,128)}, f32[4,1,320]{2,1,0:T(1,128)}, f32[4,1,256]{2,1,0:T(1,128)}) custom-call(bf16[4,64,1024]{2,1,0:T(8,128)(2,1)} %bitcast.105, bf16[4,16,1024]{2,1,0:T(8,128)(2,1)} %bitcast.114, f32[5,1024]{1,0:T(8,128)} %pad_maximum_fusion.2.refs_2_, ...), custom_call_target="tpu_custom_call" | custom-call | tf_op jit(solution)/shard_map/exchange_1/pallas_call | solution.py:273
  42.3 0.7 fusion.42
  43.1 0.7 slice_reduce_fusion.1
  43.9 1.5 reduce_sum.62.refs_2_
  45.5 1.0 copy.28
  46.5 1.0 copy.29
  47.5 1.3 copy.30
  48.8 35.0 %exchange_2.1 = (bf16[4,4,64,1024]{3,2,1,0:T(8,128)(2,1)}, bf16[4,4,16,1024]{3,2,1,0:T(8,128)(2,1)}, f32[4,5,1024]{2,1,0:T(8,128)}) custom-call(bf16[4,64,1024]{2,1,0:T(8,128)(2,1)} %get-tuple-element.15.refs_0_, bf16[4,16,1024]{2,1,0:T(8,128)(2,1)} %get-tuple-element.16.refs_1_, f32[5,1024]{1,0:T(8,128)} %reduce_sum.62.refs_2_), custom_call_target="tpu_custom_call" | custom-call | tf_op jit(solution)/shard_map/exchange_2/pallas_call | solution.py:273
  83.8 0.8 dynamic-slice.2
  84.6 1.0 dynamic-slice_add_fusion.1
  85.6 1.4 add_convert_fusion.2
  86.9 1.9 copy.27
  89.4 1.0 convolution_convert_fusion.1.refs_1_
  90.4 0.8 add_convert_fusion
  91.3 4.5 %fusion.2.refs_0_ = bf16[4,1280,256]{2,1,0:T(8,128)(2,1)} fusion(bf16[256,1024]{1,0:T(8,128)(2,1)S(1)} %fusion.14, bf16[1024,1024]{1,0:T(8,128)(2,1)S(1)} %add_convert_fusion, bf16[1024,4,128]{0,2,1:T(8,128)(2,1)S(1)} %bitcast.108, bf16[1024,4,64]{0,2,1:T(8,128)(2,1)S(1)} %bitcast.111, bf16[1024,4,64]{0,2,1:T(8,128)(2,1)S(1)} %bitcast.110), kind=kOutput, calls=%fused_computation.7 | convolution fusion | flops 2697199616 | bytes 7340032 | tf_op jit(solution)/shard_map/tk,hkc->htc/dot_general | solution.py:488
  95.7 69.6 %exchange_3.1 = (bf16[4,1280,256]{2,1,0:T(8,128)(2,1)}, bf16[4,320,128]{2,1,0:T(8,128)(2,1)}) custom-call(bf16[4,1280,256]{2,1,0:T(8,128)(2,1)} %fusion.2.refs_0_, bf16[320,128]{1,0:T(8,128)(2,1)} %convolution_convert_fusion.1.refs_1_), custom_call_target="tpu_custom_call" | custom-call | tf_op jit(solution)/shard_map/exchange_3/pallas_call | solution.py:273
  165.3 3.2 reduce_sum.63
  168.5 0.7 reduce_sum.64.refs_0_
  169.2 1.6 slice.115.ck_ref
  170.7 1.5 slice.116.cv_ref
  172.2 7.2 %exchange_4.1 = bf16[4,320,128]{2,1,0:T(8,128)(2,1)} custom-call(bf16[320,128]{1,0:T(8,128)(2,1)} %reduce_sum.64.refs_0_), custom_call_target="tpu_custom_call" | custom-call | tf_op jit(solution)/shard_map/exchange_4/pallas_call | solution.py:273
  179.4 0.9 slice.95
  180.2 1.0 slice.94
  181.2 1.7 slice.110.v_ref
  182.9 1.9 fusion.41
  187.4 1.2 slice_add_fusion
  188.6 21.6 %mix.1.refs_0_ = bf16[1024,128]{1,0:T(8,128)(2,1)} custom-call(bf16[1024,64]{1,0:T(8,128)(2,1)} %get-tuple-element.26.q_ref, bf16[1024,64]{1,0:T(8,128)(2,1)} %get-tuple-element.25.k_ref, bf16[1024,128]{1,0:T(8,128)(2,1)} %slice.110.v_ref, f32[1024,64]{1,0:T(8,128)} %get-tuple-element.38.f_ref, f32[1024,64]{1,0:T(8,128)} %get-tuple-element.37.b_ref, ...), custom_call_target="tpu_custom_call" | custom-call | tf_op jit(solution)/shard_map/mix/pallas_call | solution.py:397
  210.2 24.2 %exchange_5.1 = bf16[4,1024,128]{2,1,0:T(8,128)(2,1)} custom-call(bf16[1024,128]{1,0:T(8,128)(2,1)} %mix.1.refs_0_), custom_call_target="tpu_custom_call" | custom-call | tf_op jit(solution)/shard_map/exchange_5/pallas_call | solution.py:273
  234.4 3.8 %bitcast_convert_fusion = bf16[1024,1024]{0,1:T(8,128)(2,1)} fusion(bf16[4,1024,128]{2,1,0:T(8,128)(2,1)} %exchange_5.1, bf16[4,128,1024]{2,1,0:T(8,128)(2,1)S(1)} %bitcast.97), kind=kOutput, calls=%fused_computation | convolution fusion | flops 1074790400 | bytes 4194304 | tf_op jit(solution)/shard_map/htc,hcd->td/dot_general | solution.py:533
  238.2 3.9 %copy.40 = bf16[1024,4,256]{2,0,1:T(8,128)(2,1)} copy(bf16[1024,4,256]{0,2,1:T(8,128)(2,1)} %bitcast.104) | data formatting | bytes 4194304 | tf_op jit(solution)/shard_map/reshape | solution.py:541
  242.2 27.2 %exchange_6.1 = bf16[4,1024,256]{2,1,0:T(8,128)(2,1)} custom-call(bf16[4,1024,256]{2,1,0:T(8,128)(2,1)} %bitcast.100), custom_call_target="tpu_custom_call" | custom-call | tf_op jit(solution)/shard_map/exchange_6/pallas_call | solution.py:273
  269.4 2.0 convert_reduce_fusion
  271.4 1.0 add_convert_fusion.1
  272.4 20.4 %exchange_7.1.refs_0_ = bf16[4,256,256]{2,1,0:T(8,128)(2,1)} custom-call(bf16[4,256,256]{2,1,0:T(8,128)(2,1)} %bitcast.107), custom_call_target="tpu_custom_call" | custom-call | tf_op jit(solution)/shard_map/exchange_7/pallas_call | solution.py:273
  292.8 25.9 %exchange_8.1 = bf16[4,4,256,256]{3,2,1,0:T(8,128)(2,1)} custom-call(bf16[4,256,256]{2,1,0:T(8,128)(2,1)} %exchange_7.1.refs_0_), custom_call_target="tpu_custom_call" | custom-call | tf_op jit(solution)/shard_map/exchange_8/pallas_call | solution.py:273
  318.7 2.8 copy.41
  321.5 2.9 copy.42
  (63 shorter events, 6.0 us)
Async XLA Ops:
  0.0 1.2 copy-start
  0.0 7.5 %copy-start.13 = (f32[1024]{0:T(1024)S(1)}, f32[1024]{0:T(1024)}, u32[]{:S(2)}) copy-start(f32[1024]{0:T(1024)} %param.18) | copy-start | bytes 12292
  0.0 7.5 %copy-start.12 = (f32[1024]{0:T(1024)S(1)}, f32[1024]{0:T(1024)}, u32[]{:S(2)}) copy-start(f32[1024]{0:T(1024)} %param.17) | copy-start | bytes 12292
  4.6 7.1 %copy-start.1 = (bf16[3,1024,1024]{2,1,0:T(8,128)(2,1)S(1)}, bf16[3,1024,1024]{2,1,0:T(8,128)(2,1)}, u32[]{:S(2)}) copy-start(bf16[3,1024,1024]{2,1,0:T(8,128)(2,1)} %param.19) | copy-start | bytes 18874372
  6.8 4.2 %copy-start.14 = (f32[256,4]{0,1:T(4,128)S(1)}, f32[256,4]{0,1:T(4,128)}, u32[]{:S(2)}) copy-start(f32[256,4]{0,1:T(4,128)} %param.27) | copy-start | bytes 12292
  11.7 3.1 copy-start.10
  12.6 32.9 %copy-start.5 = (bf16[1024,256]{1,0:T(8,128)(2,1)S(1)}, bf16[1024,256]{1,0:T(8,128)(2,1)}, u32[]{:S(2)}) copy-start(bf16[1024,256]{1,0:T(8,128)(2,1)} %param.21) | copy-start | bytes 1572868
  12.6 33.9 %copy-start.6 = (bf16[1024,256]{1,0:T(8,128)(2,1)S(1)}, bf16[1024,256]{1,0:T(8,128)(2,1)}, u32[]{:S(2)}) copy-start(bf16[1024,256]{1,0:T(8,128)(2,1)} %param.22) | copy-start | bytes 1572868
  14.8 32.7 %copy-start.2 = (bf16[1024,512]{1,0:T(8,128)(2,1)S(1)}, bf16[1024,512]{1,0:T(8,128)(2,1)}, u32[]{:S(2)}) copy-start(bf16[1024,512]{1,0:T(8,128)(2,1)} %param.23) | copy-start | bytes 3145732
  85.6 3.2 copy-start.4
  89.4 1.8 copy-start.3
  89.4 1.8 copy-start.7
  89.4 1.8 copy-start.8
  165.3 3.2 copy-start.9
  168.5 16.4 %copy-start.15 = (bf16[2,64,256]{2,1,0:T(8,128)(2,1)S(1)}, bf16[2,64,256]{2,1,0:T(8,128)(2,1)}, u32[]{:S(2)}) copy-start(bf16[2,64,256]{2,1,0:T(8,128)(2,1)} %param.25) | copy-start | bytes 196612
  184.8 2.6 copy-start.11

commit v2 on v1

--- a/solution.py
+++ b/solution.py
@@ -283,6 +283,137 @@
         compiler_params=pltpu.CompilerParams(collective_id=collective, has_side_effects=True),
         name=f"exchange_{collective}",
     )(*arrays)
+
+
+def relay_kernel(across, along, items, *refs):
+    total = len(items)
+    sources, targets = refs[:total], refs[total : 2 * total]
+    own_sem, far_send, far_recv, near_send, near_recv, pass_send, pass_recv = refs[2 * total :]
+    far, near = lax.axis_size(across), lax.axis_size(along)
+    here, mine = lax.axis_index(across), lax.axis_index(along)
+    pairs = near // 2
+    partner = mine + 1 - 2 * lax.rem(mine, 2)
+    barrier = pltpu.get_barrier_semaphore()
+    for step in range(1, far):
+        pl.semaphore_signal(
+            barrier, inc=1, device_id={across: lax.rem(here + step, far)}, device_id_type=MESH
+        )
+    pl.semaphore_signal(barrier, inc=1, device_id={along: partner}, device_id_type=MESH)
+    for step in range(1, pairs):
+        pl.semaphore_signal(
+            barrier, inc=1, device_id={along: lax.rem(mine + 2 * step, near)}, device_id_type=MESH
+        )
+    pl.semaphore_wait(barrier, far - 1 + pairs)
+
+    def view(item, source, holder):
+        scatter, forward, block = items[item]
+        target = targets[item]
+        if not forward:
+            return target.at[source]
+        if block is None:
+            return target.at[source, holder]
+        start = pl.multiple_of((source * near + holder) * block, block)
+        return target.at[:, pl.ds(start, block)]
+
+    def taken(item, peer):
+        return sources[item].at[peer] if items[item][0] else sources[item]
+
+    first, sent, arrive = {}, [], []
+    for item in range(total):
+        copy = pltpu.make_async_copy(taken(item, here), view(item, here, mine), own_sem.at[item])
+        copy.start()
+        first[item, 0] = copy
+        for step in range(1, far):
+            peer = lax.rem(here + step, far)
+            copy = pltpu.make_async_remote_copy(
+                src_ref=taken(item, peer),
+                dst_ref=view(item, here, mine),
+                send_sem=far_send.at[item, step],
+                recv_sem=far_recv.at[item, step],
+                device_id={across: peer},
+                device_id_type=MESH,
+            )
+            copy.start()
+            first[item, step] = copy
+            sent.append(copy)
+
+    def hand(item, step, block, slot, sends, recvs, peer):
+        copy = pltpu.make_async_remote_copy(
+            src_ref=block,
+            dst_ref=block,
+            send_sem=sends.at[item, step, slot],
+            recv_sem=recvs.at[item, step, slot],
+            device_id={along: peer},
+            device_id_type=MESH,
+        )
+        copy.start()
+        sent.append(copy)
+        return copy
+
+    crossed = []
+
+    def pass_on():
+        for item, step, source, slot, copy in crossed:
+            copy.wait_recv()
+            holder = lax.rem(mine + near - 2 * slot, near)
+            block = view(item, source, holder)
+            arrive.append(hand(item, step, block, slot, pass_send, pass_recv, partner))
+        crossed.clear()
+
+    for step in range(far):
+        source = lax.rem(here - step + far, far)
+        fresh = []
+        for item in range(total):
+            if not items[item][1]:
+                continue
+            if step:
+                first[item, step].wait_recv()
+            else:
+                first[item, step].wait()
+            block = view(item, source, mine)
+            for slot in range(1, pairs):
+                peer = lax.rem(mine + 2 * slot, near)
+                copy = hand(item, step, block, slot, near_send, near_recv, peer)
+                fresh.append((item, step, source, slot, copy))
+            arrive.append(hand(item, step, block, 0, near_send, near_recv, partner))
+        pass_on()
+        crossed.extend(fresh)
+    pass_on()
+    for item in range(total):
+        if not items[item][1]:
+            first[item, 0].wait()
+            for step in range(1, far):
+                first[item, step].wait_recv()
+    for copy in arrive:
+        copy.wait_recv()
+    for copy in sent:
+        copy.wait_send()
+
+
+def relay(across, along, collective, *items):
+    far, near = lax.axis_size(across), lax.axis_size(along)
+    shapes = []
+    for array, scatter, forward, block in items:
+        shape = array.shape[1:] if scatter else array.shape
+        if block is not None:
+            full = (shape[0], far * near * block)
+        elif forward:
+            full = (far, near) + shape
+        else:
+            full = (far,) + shape
+        shapes.append(jax.ShapeDtypeStruct(full, array.dtype))
+    dma = pltpu.SemaphoreType.DMA
+    count, pairs = len(items), near // 2
+    return pl.pallas_call(
+        functools.partial(relay_kernel, across, along, tuple(i[1:] for i in items)),
+        out_shape=shapes,
+        in_specs=[pl.BlockSpec(memory_space=pltpu.VMEM)] * count,
+        out_specs=[pl.BlockSpec(memory_space=pltpu.VMEM)] * count,
+        scratch_shapes=[dma((count,)), dma((count, far)), dma((count, far))]
+        + [dma((count, far, pairs))] * 4,
+        compiler_params=pltpu.CompilerParams(collective_id=collective, has_side_effects=True),
+        name=f"relay_{collective}",
+    )(*[item[0] for item in items])
 
 
 def narrow_dot(left, right, dims):
@@ -448,27 +579,21 @@
         own = lax.dynamic_slice_in_dim(tokens, at_tp * quarter, quarter, 0)
         return own.reshape(quarter, sp, inner).transpose(1, 0, 2)
 
-    latent_share, context_share, terms_all, scales_all, shift_all = exchange(
+    terms_all, latent_all, context_all, scales_all, shift_all = relay(
         "sp",
+        "tp",
         1,
-        (share(latent), True),
-        (share(context), True),
-        (terms, False),
-        (scales, False),
-        (decay_shift.T[:, None, :], True),
-    )
-    latent_all, context_all, modulation = exchange(
-        "tp",
-        2,
-        (latent_share, False),
-        (context_share, False),
-        (jnp.sum(terms_all, axis=0), False),
-    )
-    modulation = modulation.transpose(1, 0, 2).reshape(terms.shape[0], model)
+        (terms, False, True, None),
+        (share(latent), True, True, None),
+        (share(context), True, True, None),
+        (scales, False, False, None),
+        (decay_shift.T[:, None, :], True, False, None),
+    )
+    modulation = jnp.sum(terms_all, axis=0).transpose(1, 0, 2).reshape(terms.shape[0], model)
     own_mod = lax.dynamic_slice_in_dim(modulation, at_sp * inner, inner, 1)
     own_gain = lax.dynamic_slice_in_dim(norm_gain, at_sp * inner, inner, 0)
-    raw_latent = latent_all.transpose(1, 0, 2, 3).reshape(sp * rows, inner)
-    raw_context = context_all.transpose(1, 0, 2, 3).reshape(sp * context_rows, inner)
+    raw_latent = latent_all.reshape(sp * rows, inner)
+    raw_context = context_all.reshape(sp * context_rows, inner)
 
     def tokens_of(raw, inverses, shift_row, scale_row):
         normalized = raw.astype(jnp.float32) * inverses.reshape(-1, 1)
@@ -499,9 +624,10 @@
         jnp.concatenate([w_rank[0], w_rank[1]], axis=1),
         preferred_element_type=jnp.float32,
     ).astype(jnp.bfloat16)
-    partial_all, rank_all = exchange("sp", 3, (partial, True), (rank_partial, False))
-    rank_own = jnp.sum(rank_all.astype(jnp.float32), axis=0).astype(jnp.bfloat16)
-    (rank_full,) = exchange("tp", 4, (rank_own, False))
+    rank_all, partial_all = relay(
+        "sp", "tp", 3, (rank_partial, False, True, None), (partial, True, False, None)
+    )
+    rank_full = jnp.sum(rank_all.astype(jnp.float32), axis=0).astype(jnp.bfloat16)
     width = rank_full.shape[-1]
     cut = rank_rows.shape[0] - sp * context_rows // tp
 
@@ -544,9 +670,8 @@
     gate = lax.dynamic_slice_in_dim(own_mod[2], at_tp * columns, columns, 0)
     residual = lax.dynamic_slice_in_dim(raw_latent, at_tp * columns, columns, 1)
     slab = (residual.astype(jnp.float32) + gate * summed).astype(jnp.bfloat16)
-    (slab_rows,) = exchange("sp", 7, (slab.reshape(sp, rows, columns), True))
-    (slab_all,) = exchange("tp", 8, (slab_rows, False))
-    return slab_all.transpose(2, 1, 0, 3).reshape(rows, model)
+    (whole_rows,) = relay("sp", "tp", 7, (slab.reshape(sp, rows, columns), True, True, columns))
+    return whole_rows
 
 
 def chosen(mesh, *arrays):

time: 328 us -> 274 us (0.84)
  Pallas kernels: 256 us -> 210 us
  local copies, waits for them, and re-layouts: 35.9 us -> 29.1 us
    pallas_call x8 -> x2, Pallas kernels: 235 us -> 63.4 us  [exchange(): pl.pallas_call(functools.partial(exchange_kernel, axis, count, sends), ou...]
    pallas_call x0 -> x3, Pallas kernels: none -> 125 us  [relay(): pl.pallas_call(functools.partial(relay_kernel, across, along, tuple((i[1:...]
    transpose x2, local copies, waits for them, and re-layouts: 4.63 us -> 0.03 us  [in_order(): tensor.reshape(tp, sp, -1, width).transpose(1, 0, 2, 3).reshape(-1, width)]
    unnamed x35 -> x34, local copies, waits for them, and re-layouts: 4.62 us -> 7.75 us
where the time goes in v2:
time: 274 us; the launch traced here: 273 us
  Pallas kernels  210 us (77%)
  local copies, waits for them, and re-layouts  29.1 us (11%)
  other arithmetic  19.1 us (7%)
  matrix products  14.3 us (5%)
    pallas_call x3, Pallas kernels, relay(): pl.pallas_call(functools.partial(relay_kernel, across, along, tuple((i[1:...  125 us
    pallas_call x2, Pallas kernels, exchange(): pl.pallas_call(functools.partial(exchange_kernel, axis, count, sends), ou...  63.4 us
    pallas_call x1, Pallas kernels, mix(): pl.pallas_call(mix_kernel, out_shape=jax.ShapeDtypeStruct((length, depth)...  21.6 us
    unnamed x34, local copies, waits for them, and re-layouts  7.75 us

profile of v2, /device:TPU:0, one launch (start us, length us, event | category | flops | bytes accessed | tf_op | source)
XLA Modules:
  0.0 272.6 jit_solution(1407003450765535637)
XLA Ops:
  0.0 1.2 copy-done
  1.2 1.3 dynamic-slice_bitcast_fusion.4.gain_ref
  2.6 1.2 multiply_reduce_fusion.1
  3.8 0.8 constant_dynamic-slice_fusion.1
  4.6 2.2 multiply_reduce_fusion
  6.9 0.6 broadcast_in_dim.6.refs_3_
  7.5 0.7 dynamic_slice.40
  8.2 2.8 %fusion = f32[1,2,1024]{2,0,1:T(1,128)S(1)} fusion(bf16[1024,1,1]{0,1,2:T(2,128)(2,1)S(1)} %reshape.120, bf16[3,1024,1024]{2,1,0:T(8,128)(2,1)} %param.19), kind=kOutput, calls=%fused_computation.4 | convolution fusion | flops 4194304 | bytes 4204544 | tf_op jit(solution)/shard_map/d,rdc->rc/dot_general | solution.py:566
  11.7 0.9 fusion.44
  12.6 0.6 pad_maximum_fusion.2.refs_0_
  13.2 1.0 constant_dynamic-slice_fusion.4
  14.2 0.7 copy.58
  15.0 1.1 constant_dynamic-slice_fusion.5
  16.0 0.8 copy.57
  16.9 1.0 copy.35
  17.9 1.0 copy.36
  18.9 1.3 copy.37
  20.2 34.4 %relay_1.1 = (f32[4,4,5,1024]{3,2,1,0:T(8,128)}, bf16[4,4,64,1024]{3,2,1,0:T(8,128)(2,1)}, bf16[4,4,16,1024]{3,2,1,0:T(8,128)(2,1)}, f32[4,1,320]{2,1,0:T(1,128)}, f32[4,1,256]{2,1,0:T(1,128)}) custom-call(f32[5,1024]{1,0:T(8,128)} %pad_maximum_fusion.2.refs_0_, bf16[4,64,1024]{2,1,0:T(8,128)(2,1)} %bitcast.96, bf16[4,16,1024]{2,1,0:T(8,128)(2,1)} %bitcast.105, ...), custom_call_target="tpu_custom_call" | custom-call | tf_op jit(solution)/shard_map/relay_1/pallas_call | solution.py:407
  54.6 1.1 reduce_sum.62
  55.8 0.7 fusion.43
  56.6 0.7 fusion.42
  57.5 1.3 add_convert_fusion.2
  58.8 1.4 fusion.14
  60.3 1.1 convert_element_type.70
  61.6 1.0 convolution_convert_fusion.1.refs_0_
  62.5 0.8 add_convert_fusion
  63.4 4.5 %fusion.2.refs_1_ = bf16[4,1280,256]{2,1,0:T(8,128)(2,1)} fusion(bf16[256,1024]{1,0:T(8,128)(2,1)S(1)} %fusion.14, bf16[1024,1024]{1,0:T(8,128)(2,1)S(1)} %add_convert_fusion, bf16[1024,4,128]{0,2,1:T(8,128)(2,1)S(1)} %bitcast.99, bf16[1024,4,64]{0,2,1:T(8,128)(2,1)S(1)} %bitcast.102, bf16[1024,4,64]{0,2,1:T(8,128)(2,1)S(1)} %bitcast.101), kind=kOutput, calls=%fused_computation.7 | convolution fusion | flops 2697199616 | bytes 7340032 | tf_op jit(solution)/shard_map/tk,hkc->htc/dot_general | solution.py:613
  67.9 61.9 %relay_3.1 = (bf16[4,4,320,128]{3,2,1,0:T(8,128)(2,1)}, bf16[4,1280,256]{2,1,0:T(8,128)(2,1)}) custom-call(bf16[320,128]{1,0:T(8,128)(2,1)} %convolution_convert_fusion.1.refs_0_, bf16[4,1280,256]{2,1,0:T(8,128)(2,1)} %fusion.2.refs_1_), custom_call_target="tpu_custom_call" | custom-call | tf_op jit(solution)/shard_map/relay_3/pallas_call | solution.py:407
  129.7 3.1 %reduce_sum.63 = bf16[1280,256]{1,0:T(8,128)(2,1)} reduce(bf16[4,1280,256]{2,1,0:T(8,128)(2,1)} %get-tuple-element.16, bf16[]{:T(256)} %constant.55.clone.1), dimensions={0}, to_apply=%region_3.4 | reduce | flops 983040 | bytes 3276802 | tf_op jit(solution)/shard_map/reduce_sum | solution.py:638
  132.9 1.6 reduce_sum.64
  134.6 1.5 slice.117.ck_ref
  136.1 1.5 slice.118.cv_ref
  137.6 1.7 slice.110.v_ref
  139.3 1.9 fusion.41
  141.2 0.6 fusion.18
  141.8 0.7 slice.120.cb_ref
  142.5 0.6 fusion.16
  143.1 0.7 slice.119.cf_ref
  143.8 1.2 slice_add_fusion
  144.9 21.6 %mix.1.refs_0_ = bf16[1024,128]{1,0:T(8,128)(2,1)} custom-call(bf16[1024,64]{1,0:T(8,128)(2,1)} %get-tuple-element.20.q_ref, bf16[1024,64]{1,0:T(8,128)(2,1)} %get-tuple-element.19.k_ref, bf16[1024,128]{1,0:T(8,128)(2,1)} %slice.110.v_ref, f32[1024,64]{1,0:T(8,128)} %get-tuple-element.32.f_ref, f32[1024,64]{1,0:T(8,128)} %get-tuple-element.31.b_ref, ...), custom_call_target="tpu_custom_call" | custom-call | tf_op jit(solution)/shard_map/mix/pallas_call | solution.py:528
  166.6 35.6 %exchange_5.1 = bf16[4,1024,128]{2,1,0:T(8,128)(2,1)} custom-call(bf16[1024,128]{1,0:T(8,128)(2,1)} %mix.1.refs_0_), custom_call_target="tpu_custom_call" | custom-call | tf_op jit(solution)/shard_map/exchange_5/pallas_call | solution.py:273
  202.1 3.8 %bitcast_convert_fusion = bf16[1024,1024]{0,1:T(8,128)(2,1)} fusion(bf16[4,1024,128]{2,1,0:T(8,128)(2,1)} %exchange_5.1, bf16[4,128,1024]{2,1,0:T(8,128)(2,1)S(1)} %bitcast.92), kind=kOutput, calls=%fused_computation | convolution fusion | flops 1074790400 | bytes 4194304 | tf_op jit(solution)/shard_map/htc,hcd->td/dot_general | solution.py:659
  206.0 4.0 %copy.44 = bf16[1024,4,256]{2,0,1:T(8,128)(2,1)} copy(bf16[1024,4,256]{0,2,1:T(8,128)(2,1)} %bitcast.95) | data formatting | bytes 4194304 | tf_op jit(solution)/shard_map/reshape | solution.py:667
  209.9 27.8 %exchange_6.1 = bf16[4,1024,256]{2,1,0:T(8,128)(2,1)} custom-call(bf16[4,1024,256]{2,1,0:T(8,128)(2,1)} %bitcast.93), custom_call_target="tpu_custom_call" | custom-call | tf_op jit(solution)/shard_map/exchange_6/pallas_call | solution.py:273
  237.8 2.0 convert_reduce_fusion
  239.8 1.0 add_convert_fusion.1
  240.8 28.6 %relay_7.1 = bf16[256,4096]{1,0:T(8,128)(2,1)} custom-call(bf16[4,256,256]{2,1,0:T(8,128)(2,1)} %bitcast.97), custom_call_target="tpu_custom_call" | custom-call | tf_op jit(solution)/shard_map/relay_7/pallas_call | solution.py:407
  269.4 3.1 %copy.62 = bf16[256,4096]{1,0:T(8,128)(2,1)} copy(bf16[256,4096]{1,0:T(8,128)(2,1)} %relay_7.1) | data formatting | bytes 4194304
  (53 shorter events, 1.3 us)
Async XLA Ops:
  0.0 1.2 copy-start
  0.0 7.5 %copy-start.12 = (f32[1024]{0:T(1024)S(1)}, f32[1024]{0:T(1024)}, u32[]{:S(2)}) copy-start(f32[1024]{0:T(1024)} %param.18) | copy-start | bytes 12292
  0.0 7.5 %copy-start.11 = (f32[1024]{0:T(1024)S(1)}, f32[1024]{0:T(1024)}, u32[]{:S(2)}) copy-start(f32[1024]{0:T(1024)} %param.17) | copy-start | bytes 12292
  4.6 7.1 %copy-start.1 = (bf16[3,1024,1024]{2,1,0:T(8,128)(2,1)S(1)}, bf16[3,1024,1024]{2,1,0:T(8,128)(2,1)}, u32[]{:S(2)}) copy-start(bf16[3,1024,1024]{2,1,0:T(8,128)(2,1)} %param.19) | copy-start | bytes 18874372
  6.8 4.2 %copy-start.13 = (f32[256,4]{0,1:T(4,128)S(1)}, f32[256,4]{0,1:T(4,128)}, u32[]{:S(2)}) copy-start(f32[256,4]{0,1:T(4,128)} %param.27) | copy-start | bytes 12292
  11.7 3.2 %copy-start.9 = (bf16[2,1024,64]{1,2,0:T(8,128)(2,1)S(1)}, bf16[2,1024,64]{1,2,0:T(8,128)(2,1)}, u32[]{:S(2)}) copy-start(bf16[2,1024,64]{1,2,0:T(8,128)(2,1)} %param.24) | copy-start | bytes 786436
  12.6 4.3 %copy-start.5 = (bf16[1024,256]{1,0:T(8,128)(2,1)S(1)}, bf16[1024,256]{1,0:T(8,128)(2,1)}, u32[]{:S(2)}) copy-start(bf16[1024,256]{1,0:T(8,128)(2,1)} %param.21) | copy-start | bytes 1572868
  12.6 5.3 %copy-start.6 = (bf16[1024,256]{1,0:T(8,128)(2,1)S(1)}, bf16[1024,256]{1,0:T(8,128)(2,1)}, u32[]{:S(2)}) copy-start(bf16[1024,256]{1,0:T(8,128)(2,1)} %param.22) | copy-start | bytes 1572868
  13.2 5.7 %copy-start.3 = (bf16[1024,512]{1,0:T(8,128)(2,1)S(1)}, bf16[1024,512]{1,0:T(8,128)(2,1)}, u32[]{:S(2)}) copy-start(bf16[1024,512]{1,0:T(8,128)(2,1)} %param.23) | copy-start | bytes 3145732
  58.8 3.7 %copy-start.2 = (bf16[4,4,64,1024]{3,2,1,0:T(8,128)(2,1)S(1)}, bf16[4,4,64,1024]{3,2,1,0:T(8,128)(2,1)}, u32[]{:S(2)}) copy-start(bf16[4,4,64,1024]{3,2,1,0:T(8,128)(2,1)} %get-tuple-element.12) | copy-start | bytes 6291460
  61.5 1.8 copy-start.4
  61.5 1.8 copy-start.7
  61.6 1.8 copy-start.8
  132.9 8.3 %copy-start.14 = (bf16[2,64,256]{2,1,0:T(8,128)(2,1)S(1)}, bf16[2,64,256]{2,1,0:T(8,128)(2,1)}, u32[]{:S(2)}) copy-start(bf16[2,64,256]{2,1,0:T(8,128)(2,1)} %param.25) | copy-start | bytes 196612
  141.2 2.6 copy-start.10

commit v3 on v2

--- a/solution.py
+++ b/solution.py
@@ -237,13 +237,27 @@
             barrier, inc=1, device_id={axis: lax.rem(me + step, count)}, device_id_type=MESH
         )
     pl.semaphore_wait(barrier, count - 1)
+
+    def columns(ref, index, width):
+        return ref.at[:, pl.ds(pl.multiple_of(index * width, width), width)]
+
+    def taken(item, peer):
+        if not sends[item]:
+            return sources[item]
+        return columns(sources[item], peer, targets[item].shape[2])
+
+    def placed(item):
+        if sends[item]:
+            return targets[item].at[me]
+        return columns(targets[item], me, sources[item].shape[1])
+
     copies = []
     for item in range(total):
         for step in range(1, count):
             peer = lax.rem(me + step, count)
             copy = pltpu.make_async_remote_copy(
-                src_ref=sources[item].at[peer] if sends[item] else sources[item],
-                dst_ref=targets[item].at[me],
+                src_ref=taken(item, peer),
+                dst_ref=placed(item),
                 send_sem=send_sem.at[item, step - 1],
                 recv_sem=recv_sem.at[item, step - 1],
                 device_id={axis: peer},
@@ -253,8 +267,8 @@
             copies.append(copy)
     for item in range(total):
         copy = pltpu.make_async_copy(
-            sources[item].at[me] if sends[item] else sources[item],
-            targets[item].at[me],
+            taken(item, me),
+            placed(item),
             own_sem.at[item],
         )
         copy.start()
@@ -268,7 +282,11 @@
     sends = tuple(scatter for _, scatter in items)
     arrays = [array for array, _ in items]
     shapes = [
-        jax.ShapeDtypeStruct(a.shape if s else (count,) + a.shape, a.dtype) for a, s in items
+        jax.ShapeDtypeStruct(
+            (count, a.shape[0], a.shape[1] // count) if s else (a.shape[0], count * a.shape[1]),
+            a.dtype,
+        )
+        for a, s in items
     ]
     return pl.pallas_call(
         functools.partial(exchange_kernel, axis, count, sends),
@@ -285,7 +303,7 @@
     )(*arrays)
 
 
-def relay_kernel(across, along, items, *refs):
+def relay_kernel(across, along, items, meanwhile, *refs):
     total = len(items)
     sources, targets = refs[:total], refs[total : 2 * total]
     own_sem, far_send, far_recv, near_send, near_recv, pass_send, pass_recv = refs[2 * total :]
@@ -336,6 +354,9 @@
             copy.start()
             first[item, step] = copy
             sent.append(copy)
+
+    if meanwhile is not None:
+        meanwhile()
 
     def hand(item, step, block, slot, sends, recvs, peer):
         copy = pltpu.make_async_remote_copy(
@@ -405,7 +426,7 @@
     dma = pltpu.SemaphoreType.DMA
     count, pairs = len(items), near // 2
     return pl.pallas_call(
-        functools.partial(relay_kernel, across, along, tuple(i[1:] for i in items)),
+        functools.partial(relay_kernel, across, along, tuple(i[1:] for i in items), None),
         out_shape=shapes,
         in_specs=[pl.BlockSpec(memory_space=pltpu.VMEM)] * count,
         out_specs=[pl.BlockSpec(memory_space=pltpu.VMEM)] * count,
@@ -414,6 +435,135 @@
         compiler_params=pltpu.CompilerParams(collective_id=collective, has_side_effects=True),
         name=f"relay_{collective}",
     )(*[item[0] for item in items])
+
+
+def join_kernel(across, along, rank_ref, part_ref, rank_out, joined_ref, *scratch):
+    relay_sems = scratch[:7]
+    buffers, sends, recvs = scratch[7:11], scratch[11], scratch[12]
+    came, gone = buffers[:2], buffers[2:]
+    count = lax.axis_size(across)
+    me = lax.axis_index(across)
+    rows = joined_ref.shape[0]
+    tiles = rows // BLOCK
+
+    def copy(side, owner, source):
+        return pltpu.make_async_remote_copy(
+            src_ref=source,
+            dst_ref=came[side].at[owner],
+            send_sem=sends.at[side, owner],
+            recv_sem=recvs.at[side, owner],
+            device_id={across: lax.rem(me + (1 if side == 0 else count - 1), count)},
+            device_id_type=MESH,
+        )
+
+    def owners(side):
+        return range(count - 1, 0, -1) if side == 0 else range(count - 1)
+
+    def first(side):
+        return me == (0 if side == 0 else count - 1)
+
+    def between(side, owner):
+        return (me > 0) & (me < owner) if side == 0 else (me < count - 1) & (me > owner)
+
+    def ends():
+        for side in range(2):
+
+            @pl.when(first(side))
+            def _():
+                for owner in owners(side):
+                    copy(side, owner, part_ref.at[owner]).start()
+
+    relay_kernel(across, along, ((False, True, None),), ends, rank_ref, rank_out, *relay_sems)
+
+    def step(side, owner):
+        @pl.when(between(side, owner))
+        def _():
+            copy(side, owner, gone[side].at[owner]).wait_recv()
+
+            def add(tile, carry):
+                span = pl.ds(pl.multiple_of(tile * BLOCK, BLOCK), BLOCK)
+                total = part_ref[owner, span, :].astype(jnp.float32) + came[side][
+                    owner, span, :
+                ].astype(jnp.float32)
+                gone[side][owner, span, :] = total.astype(jnp.bfloat16)
+                return carry
+
+            lax.fori_loop(0, tiles, add, 0)
+            copy(side, owner, gone[side].at[owner]).start()
+
+    def all_steps(sides):
+        for turn in range(count - 1):
+            for side in sides:
+                step(side, owners(side)[turn])
+
+    lower = me < count // 2
+
+    @pl.when(lower)
+    def _():
+        all_steps((0, 1))
+
+    @pl.when(jnp.logical_not(lower))
+    def _():
+        all_steps((1, 0))
+
+    def collect(use):
+        for side in range(2):
+            if use[side]:
+                copy(side, me, gone[side].at[me]).wait_recv()
+
+        def add(tile, carry):
+            span = pl.ds(pl.multiple_of(tile * BLOCK, BLOCK), BLOCK)
+            total = part_ref[me, span, :].astype(jnp.float32)
+            for side in range(2):
+                if use[side]:
+                    total = total + came[side][me, span, :].astype(jnp.float32)
+            joined_ref[span, :] = total.astype(jnp.bfloat16)
+            return carry
+
+        lax.fori_loop(0, tiles, add, 0)
+
+    @pl.when(first(0))
+    def _():
+        collect((False, True))
+
+    @pl.when(first(1))
+    def _():
+        collect((True, False))
+
+    @pl.when((me > 0) & (me < count - 1))
+    def _():
+        collect((True, True))
+
+    for side in range(2):
+        for owner in owners(side):
+
+            @pl.when(between(side, owner))
+            def _():
+                copy(side, owner, gone[side].at[owner]).wait_send()
+
+            @pl.when(first(side))
+            def _():
+                copy(side, owner, part_ref.at[owner]).wait_send()
+
+
+def join(across, along, collective, rank, partial):
+    far, near = lax.axis_size(across), lax.axis_size(along)
+    dma = pltpu.SemaphoreType.DMA
+    return pl.pallas_call(
+        functools.partial(join_kernel, across, along),
+        out_shape=[
+            jax.ShapeDtypeStruct((far, near) + rank.shape, rank.dtype),
+            jax.ShapeDtypeStruct(partial.shape[1:], partial.dtype),
+        ],
+        in_specs=[pl.BlockSpec(memory_space=pltpu.VMEM)] * 2,
+        out_specs=[pl.BlockSpec(memory_space=pltpu.VMEM)] * 2,
+        scratch_shapes=[dma((1,)), dma((1, far)), dma((1, far))]
+        + [dma((1, far, near // 2))] * 4
+        + [pltpu.VMEM(partial.shape, partial.dtype)] * 4
+        + [dma((2, far)), dma((2, far))],
+        compiler_params=pltpu.CompilerParams(collective_id=collective, has_side_effects=True),
+        name="join",
+    )(rank, partial)
 
 
 def narrow_dot(left, right, dims):
@@ -624,9 +774,7 @@
         jnp.concatenate([w_rank[0], w_rank[1]], axis=1),
         preferred_element_type=jnp.float32,
     ).astype(jnp.bfloat16)
-    rank_all, partial_all = relay(
-        "sp", "tp", 3, (rank_partial, False, True, None), (partial, True, False, None)
-    )
+    rank_all, joined = join("sp", "tp", 3, rank_partial, partial)
     rank_full = jnp.sum(rank_all.astype(jnp.float32), axis=0).astype(jnp.bfloat16)
     width = rank_full.shape[-1]
     cut = rank_rows.shape[0] - sp * context_rows // tp
@@ -635,7 +783,6 @@
         return tensor.reshape(tp, sp, -1, width).transpose(1, 0, 2, 3).reshape(-1, width)
 
     ranks = jnp.concatenate([in_order(rank_full[:, :cut]), in_order(rank_full[:, cut:])], axis=0)
-    joined = jnp.sum(partial_all.astype(jnp.float32), axis=0).astype(jnp.bfloat16)
     own_decay = lax.dynamic_slice_in_dim(w_decay, at_sp * DK, DK, 2)
     own_bias = lax.dynamic_slice_in_dim(decay_bias, at_sp * DK, DK, 1)
     half = width // 2
@@ -656,16 +803,9 @@
         lax.dynamic_slice_in_dim(out_gain, at_sp * DV, DV, 0)[None],
     )
     (normed_all,) = exchange("sp", 5, (normed, False))
-    part = jnp.einsum(
-        "htc,hcd->td",
-        normed_all,
-        w_out.reshape(heads, DV, -1),
-        preferred_element_type=jnp.float32,
-    ).astype(jnp.bfloat16)
+    part = jnp.dot(normed_all, w_out, preferred_element_type=jnp.float32).astype(jnp.bfloat16)
     columns = part.shape[1] // tp
-    (part_all,) = exchange(
-        "tp", 6, (part.reshape(span, tp, columns).transpose(1, 0, 2), True)
-    )
+    (part_all,) = exchange("tp", 6, (part, True))
     summed = jnp.sum(part_all.astype(jnp.float32), axis=0)
     gate = lax.dynamic_slice_in_dim(own_mod[2], at_tp * columns, columns, 0)
     residual = lax.dynamic_slice_in_dim(raw_latent, at_tp * columns, columns, 1)

time: 274 us -> 250 us (0.912)
  Pallas kernels: 210 us -> 194 us
  local copies, waits for them, and re-layouts: 29.1 us -> 23.9 us
  other arithmetic: 19.1 us -> 15.9 us
    pallas_call x3 -> x2, Pallas kernels: 125 us -> 62.9 us  [relay(): pl.pallas_call(functools.partial(relay_kernel, across, along, tuple((i[1:...]
    pallas_call x0 -> x1, Pallas kernels: none -> 61.5 us  [join(): pl.pallas_call(functools.partial(join_kernel, across, along), out_shape=[...]
    pallas_call x2, Pallas kernels: 63.4 us -> 48 us  [exchange(): pl.pallas_call(functools.partial(exchange_kernel, axis, count, sends), ou...]
    reshape x1 -> x0, local copies, waits for them, and re-layouts: 3.96 us -> none  [local_heads(): part.reshape(span, tp, columns).transpose(1, 0, 2)]
    reduce_sum x1 -> x0, other arithmetic: 3.14 us -> none  [local_heads(): jnp.sum(partial_all.astype(jnp.float32), axis=0).astype(jnp.bfloat16)]
where the time goes in v3:
time: 250 us; the launch traced here: 248 us
  Pallas kernels  194 us (78%)
  local copies, waits for them, and re-layouts  23.9 us (10%)
  other arithmetic  15.9 us (6%)
  matrix products  14.2 us (6%)
    pallas_call x2, Pallas kernels, relay(): pl.pallas_call(functools.partial(relay_kernel, across, along, tuple((i[1:...  62.9 us
    pallas_call x1, Pallas kernels, join(): pl.pallas_call(functools.partial(join_kernel, across, along), out_shape=[...  61.5 us
    pallas_call x2, Pallas kernels, exchange(): pl.pallas_call(functools.partial(exchange_kernel, axis, count, sends), ou...  48 us
    pallas_call x1, Pallas kernels, mix(): pl.pallas_call(mix_kernel, out_shape=jax.ShapeDtypeStruct((length, depth)...  21.6 us
    unnamed x34, local copies, waits for them, and re-layouts  6.52 us

profile of v3, /device:TPU:0, one launch (start us, length us, event | category | flops | bytes accessed | tf_op | source)
XLA Modules:
  0.0 248.4 jit_solution(1949134867590253772)
XLA Ops:
  0.0 1.4 dynamic-slice_bitcast_fusion.4.gain_ref
  1.4 1.2 multiply_reduce_fusion.1
  2.6 0.8 constant_dynamic-slice_fusion.1
  3.4 2.2 multiply_reduce_fusion
  5.7 0.6 broadcast_in_dim.6.refs_3_
  6.3 0.7 dynamic_slice.40
  7.0 2.8 %fusion = f32[1,2,1024]{2,0,1:T(1,128)S(1)} fusion(bf16[1024,1,1]{0,1,2:T(2,128)(2,1)S(1)} %reshape.112, bf16[3,1024,1024]{2,1,0:T(8,128)(2,1)} %param.19), kind=kOutput, calls=%fused_computation.3 | convolution fusion | flops 4194304 | bytes 4204544 | tf_op jit(solution)/shard_map/d,rdc->rc/dot_general | solution.py:716
  9.9 0.6 broadcast_in_dim.7.refs_4_
  10.5 0.9 fusion.44
  11.4 0.6 pad_maximum_fusion.2.refs_0_
  12.0 1.0 constant_dynamic-slice_fusion.4
  13.0 0.7 copy.52
  13.7 1.1 constant_dynamic-slice_fusion.5
  14.8 0.8 copy.51
  15.6 1.0 copy.32
  16.6 1.0 copy.33
  17.6 1.3 copy.34
  19.0 34.3 %relay_1.1 = (f32[4,4,5,1024]{3,2,1,0:T(8,128)}, bf16[4,4,64,1024]{3,2,1,0:T(8,128)(2,1)}, bf16[4,4,16,1024]{3,2,1,0:T(8,128)(2,1)}, f32[4,1,320]{2,1,0:T(1,128)}, f32[4,1,256]{2,1,0:T(1,128)}) custom-call(f32[5,1024]{1,0:T(8,128)} %pad_maximum_fusion.2.refs_0_, bf16[4,64,1024]{2,1,0:T(8,128)(2,1)} %bitcast.88, bf16[4,16,1024]{2,1,0:T(8,128)(2,1)} %bitcast.97, ...), custom_call_target="tpu_custom_call" | custom-call | tf_op jit(solution)/shard_map/relay_1/pallas_call | solution.py:428
  53.3 1.1 reduce_sum.50
  54.5 0.1 dynamic-slice_add_fusion.1
  54.6 0.7 fusion.43
  55.3 0.7 fusion.42
  56.2 1.3 add_convert_fusion.2
  57.5 1.4 fusion.14
  59.0 1.1 convert_element_type.68
  60.1 0.1 fusion.31
  60.3 1.0 convolution_convert_fusion.2.rank_ref
  61.3 0.8 add_convert_fusion
  62.1 4.4 %fusion.2.part_ref = bf16[4,1280,256]{2,1,0:T(8,128)(2,1)} fusion(bf16[256,1024]{1,0:T(8,128)(2,1)S(1)} %fusion.14, bf16[1024,1024]{1,0:T(8,128)(2,1)S(1)} %add_convert_fusion, bf16[1024,4,128]{0,2,1:T(8,128)(2,1)S(1)} %bitcast.91, bf16[1024,4,64]{0,2,1:T(8,128)(2,1)S(1)} %bitcast.94, bf16[1024,4,64]{0,2,1:T(8,128)(2,1)S(1)} %bitcast.93), kind=kOutput, calls=%fused_computation.6 | convolution fusion | flops 2697199616 | bytes 7340032 | tf_op jit(solution)/shard_map/tk,hkc->htc/dot_general | solution.py:763
  66.6 61.5 %join.1 = (bf16[4,4,320,128]{3,2,1,0:T(8,128)(2,1)}, bf16[1280,256]{1,0:T(8,128)(2,1)}) custom-call(bf16[320,128]{1,0:T(8,128)(2,1)} %convolution_convert_fusion.2.rank_ref, bf16[4,1280,256]{2,1,0:T(8,128)(2,1)} %fusion.2.part_ref), custom_call_target="tpu_custom_call" | custom-call | tf_op jit(solution)/shard_map/join/pallas_call | solution.py:552
  128.1 1.6 reduce_sum.51
  129.8 1.5 slice.104.ck_ref
  131.3 1.5 slice.105.cv_ref
  132.8 1.7 slice.93.v_ref
  134.5 2.0 fusion.41
  136.4 0.6 fusion.18
  137.1 0.7 slice.115.cb_ref
  137.7 0.6 fusion.16
  138.3 0.7 slice.114.cf_ref
  139.0 1.2 slice_add_fusion
  140.2 21.6 %mix.1.refs_0_ = bf16[1024,128]{1,0:T(8,128)(2,1)} custom-call(bf16[1024,64]{1,0:T(8,128)(2,1)} %get-tuple-element.20.q_ref, bf16[1024,64]{1,0:T(8,128)(2,1)} %get-tuple-element.19.k_ref, bf16[1024,128]{1,0:T(8,128)(2,1)} %slice.93.v_ref, f32[1024,64]{1,0:T(8,128)} %get-tuple-element.32.f_ref, f32[1024,64]{1,0:T(8,128)} %get-tuple-element.31.b_ref, ...), custom_call_target="tpu_custom_call" | custom-call | tf_op jit(solution)/shard_map/mix/pallas_call | solution.py:678
  161.8 21.6 %exchange_5.1 = bf16[1024,512]{1,0:T(8,128)(2,1)} custom-call(bf16[1024,128]{1,0:T(8,128)(2,1)} %mix.1.refs_0_), custom_call_target="tpu_custom_call" | custom-call | tf_op jit(solution)/shard_map/exchange_5/pallas_call | solution.py:291
  183.4 3.8 %convolution_convert_fusion.1.refs_0_ = bf16[1024,1024]{1,0:T(8,128)(2,1)} fusion(bf16[1024,512]{1,0:T(8,128)(2,1)} %exchange_5.1, bf16[512,1024]{1,0:T(8,128)(2,1)S(1)} %copy-done), kind=kOutput, calls=%fused_computation.21 | convolution fusion | flops 1074790400 | bytes 4194304 | tf_op jit(solution)/shard_map/dot_general | solution.py:806
  187.2 26.4 %exchange_6.1 = bf16[4,1024,256]{2,1,0:T(8,128)(2,1)} custom-call(bf16[1024,1024]{1,0:T(8,128)(2,1)} %convolution_convert_fusion.1.refs_0_), custom_call_target="tpu_custom_call" | custom-call | tf_op jit(solution)/shard_map/exchange_6/pallas_call | solution.py:291
  213.6 2.0 convert_reduce_fusion
  215.6 1.0 add_convert_fusion.1
  216.6 28.6 %relay_7.1 = bf16[256,4096]{1,0:T(8,128)(2,1)} custom-call(bf16[4,256,256]{2,1,0:T(8,128)(2,1)} %bitcast.89), custom_call_target="tpu_custom_call" | custom-call | tf_op jit(solution)/shard_map/relay_7/pallas_call | solution.py:428
  245.3 3.1 %copy.56 = bf16[256,4096]{1,0:T(8,128)(2,1)} copy(bf16[256,4096]{1,0:T(8,128)(2,1)} %relay_7.1) | data formatting | bytes 4194304
  (51 shorter events, 0.5 us)
Async XLA Ops:
  0.0 183.4 %copy-start = (bf16[512,1024]{1,0:T(8,128)(2,1)S(1)}, bf16[512,1024]{1,0:T(8,128)(2,1)}, u32[]{:S(2)}) copy-start(bf16[512,1024]{1,0:T(8,128)(2,1)} %param.29) | copy-start | bytes 3145732
  0.0 6.3 %copy-start.12 = (f32[1024]{0:T(1024)S(1)}, f32[1024]{0:T(1024)}, u32[]{:S(2)}) copy-start(f32[1024]{0:T(1024)} %param.18) | copy-start | bytes 12292
  0.0 6.2 %copy-start.11 = (f32[1024]{0:T(1024)S(1)}, f32[1024]{0:T(1024)}, u32[]{:S(2)}) copy-start(f32[1024]{0:T(1024)} %param.17) | copy-start | bytes 12292
  3.4 7.0 %copy-start.1 = (bf16[3,1024,1024]{2,1,0:T(8,128)(2,1)S(1)}, bf16[3,1024,1024]{2,1,0:T(8,128)(2,1)}, u32[]{:S(2)}) copy-start(bf16[3,1024,1024]{2,1,0:T(8,128)(2,1)} %param.19) | copy-start | bytes 18874372
  5.6 4.2 %copy-start.13 = (f32[256,4]{0,1:T(4,128)S(1)}, f32[256,4]{0,1:T(4,128)}, u32[]{:S(2)}) copy-start(f32[256,4]{0,1:T(4,128)} %param.27) | copy-start | bytes 12292
  10.5 3.2 %copy-start.9 = (bf16[2,1024,64]{1,2,0:T(8,128)(2,1)S(1)}, bf16[2,1024,64]{1,2,0:T(8,128)(2,1)}, u32[]{:S(2)}) copy-start(bf16[2,1024,64]{1,2,0:T(8,128)(2,1)} %param.24) | copy-start | bytes 786436
  11.4 4.2 %copy-start.5 = (bf16[1024,256]{1,0:T(8,128)(2,1)S(1)}, bf16[1024,256]{1,0:T(8,128)(2,1)}, u32[]{:S(2)}) copy-start(bf16[1024,256]{1,0:T(8,128)(2,1)} %param.21) | copy-start | bytes 1572868
  11.4 5.2 %copy-start.6 = (bf16[1024,256]{1,0:T(8,128)(2,1)S(1)}, bf16[1024,256]{1,0:T(8,128)(2,1)}, u32[]{:S(2)}) copy-start(bf16[1024,256]{1,0:T(8,128)(2,1)} %param.22) | copy-start | bytes 1572868
  12.0 5.6 %copy-start.3 = (bf16[1024,512]{1,0:T(8,128)(2,1)S(1)}, bf16[1024,512]{1,0:T(8,128)(2,1)}, u32[]{:S(2)}) copy-start(bf16[1024,512]{1,0:T(8,128)(2,1)} %param.23) | copy-start | bytes 3145732
  57.5 3.7 %copy-start.2 = (bf16[4,4,64,1024]{3,2,1,0:T(8,128)(2,1)S(1)}, bf16[4,4,64,1024]{3,2,1,0:T(8,128)(2,1)}, u32[]{:S(2)}) copy-start(bf16[4,4,64,1024]{3,2,1,0:T(8,128)(2,1)} %get-tuple-element.12) | copy-start | bytes 6291460
  60.3 1.8 copy-start.4
  60.3 1.8 copy-start.7
  60.3 1.8 copy-start.8
  128.1 8.3 %copy-start.14 = (bf16[2,64,256]{2,1,0:T(8,128)(2,1)S(1)}, bf16[2,64,256]{2,1,0:T(8,128)(2,1)}, u32[]{:S(2)}) copy-start(bf16[2,64,256]{2,1,0:T(8,128)(2,1)} %param.25) | copy-start | bytes 196612
  136.4 2.6 %copy-start.10 = (f32[4,1,256]{2,1,0:T(1,128)S(1)}, f32[4,1,256]{2,1,0:T(1,128)}, u32[]{:S(2)}) copy-start(f32[4,1,256]{2,1,0:T(1,128)} %get-tuple-element.18) | copy-start | bytes 12292
